TPU v7x, 256 devices: a whole 4x4x8 slice. The times are simulated.
256 devices in a mesh: sp: 32 (over z, y), fs: 4 (over x), tp: 2 (over core).
Axes of the slice: x: 4, y: 4, z: 8, core: 2. Of those that a mesh axis runs over, the one named last changes fastest.
Arguments:
- tokens: bfloat16 [8, 6144, 2048], P(('fs', 'tp'), 'sp'), may hold values from -6 to 6
- linear_query: bfloat16 [2048, 512], P(('sp', 'tp'), 'fs'), may hold values from -0.125 to 0.125
- linear_key: bfloat16 [2048, 512], P(('sp', 'tp'), 'fs'), may hold values from -0.125 to 0.125
- linear_decay: bfloat16 [2048, 512], P(('sp', 'tp'), 'fs'), may hold values from -0.25 to 0.25
- linear_value: bfloat16 [2048, 1024], P(('sp', 'tp'), 'fs'), may hold values from -0.125 to 0.125
- linear_gate: bfloat16 [2048, 1024], P(('sp', 'tp'), 'fs'), may hold values from -0.125 to 0.125
- decay_bias: float32 [512], P('fs'), may hold values from 2 to 5.5
- norm_gain: float32 [256], replicated, may hold values from 0.1 to 1.9
- window_query: bfloat16 [2048, 1024], P(('sp', 'tp'), 'fs'), may hold values from -0.125 to 0.125
- window_key: bfloat16 [2048, 256], P(('sp', 'tp'), 'fs'), may hold values from -0.125 to 0.125
- window_value: bfloat16 [2048, 256], P(('sp', 'tp'), 'fs'), may hold values from -0.5 to 0.5
- sink_logit: float32 [16], P('fs'), may hold values from 3 to 7
- linear_output: bfloat16 [1024, 2048], P('fs'), may hold values from -0.1875 to 0.1875
- window_output: bfloat16 [1024, 2048], P('fs'), may hold values from -0.1875 to 0.1875
Outputs:
- mixed: bfloat16 [8, 6144, 2048], P(('fs', 'tp'), 'sp')
All inputs are finite; a program needn't handle non-finite values.
Results may differ from a plain program's by a relative error of at most 0.025.
Values may be sent and summed in bfloat16 or wider, within the bound.
A program may use at most 64 MiB of HBM per device.

v0:
```python
import functools

import jax
import jax.numpy as jnp
from jax import lax
from jax.experimental import pallas as pl
from jax.experimental.pallas import tpu as pltpu
from jax.sharding import PartitionSpec as P

GLA_KEY = 128
GLA_VALUE = 256
HEAD_DIM = 64
WINDOW = 128

norm_epsilon = 1e-05
MESH = pl.DeviceIdType.MESH
f32, bf16 = jnp.float32, jnp.bfloat16


def dot(a, b):
    return jnp.dot(a, b, preferred_element_type=f32)


def dot_t(a, b):
    return lax.dot_general(a, b, (((1,), (1,)), ((), ())), preferred_element_type=f32)


def dot_rows(a, b):
    return lax.dot_general(a, b, (((0,), (0,)), ((), ())), preferred_element_type=f32)


def kernel(
    NZ, NF, NT, levels,
    tok, w1, w2, w3, bias, gain, sink, out_w,
    out,
    toks, W1, W2, W3, sums, fhi, flo, kkey, val, kvbuf, qs, oacc, state_in, state_out,
    rows, part, rbuf,
    loc_sem, wsend, wrecv, fsend, frecv, tsend, trecv, ssend, srecv, hsend, hrecv, psend, precv,
):
    z, f, t = lax.axis_index("sp"), lax.axis_index("fs"), lax.axis_index("tp")
    length = tok.shape[0]
    tau = NZ * length // 16

    barrier = pltpu.get_barrier_semaphore()
    for d in range(1, NZ):
        pl.semaphore_signal(barrier, inc=1, device_id={"sp": lax.rem(z + d, NZ)}, device_id_type=MESH)
    for d in range(1, NF):
        pl.semaphore_signal(barrier, inc=1, device_id={"fs": lax.rem(f + d, NF)}, device_id_type=MESH)
    for d in range(1, NT):
        pl.semaphore_signal(barrier, inc=1, device_id={"tp": lax.rem(t + d, NT)}, device_id_type=MESH)
    pl.semaphore_wait(barrier, NZ + NF + NT - 3)

    own = z * NT + t
    groups = ((w1, W1), (w2, W2), (w3, W3))

    def token_copy(d):
        return pltpu.make_async_remote_copy(
            src_ref=tok, dst_ref=toks.at[f], send_sem=tsend.at[d], recv_sem=trecv.at[d],
            device_id={"fs": lax.rem(f + d, NF)}, device_id_type=MESH)

    def weight_copy(g, d):
        src, dst = groups[g]
        return pltpu.make_async_remote_copy(
            src_ref=src, dst_ref=dst.at[own], send_sem=wsend.at[g, d], recv_sem=wrecv.at[g, d],
            device_id={"sp": lax.rem(z + d, NZ)}, device_id_type=MESH)

    def forward_copy(g, d, e):
        src, dst = groups[g]
        slot = lax.rem(z - d + NZ, NZ) * NT + t
        return pltpu.make_async_remote_copy(
            src_ref=src if d == 0 else dst.at[slot], dst_ref=dst.at[slot],
            send_sem=fsend.at[g, d, e], recv_sem=frecv.at[g, d, e],
            device_id={"tp": lax.rem(t + e, NT)}, device_id_type=MESH)

    for d in range(1, NF):
        token_copy(d).start()
    for g in range(3):
        for d in range(1, NZ):
            weight_copy(g, d).start()
        for e in range(1, NT):
            forward_copy(g, 0, e).start()
    local = [pltpu.make_async_copy(tok, toks.at[f], loc_sem.at[0])]
    for g in range(3):
        local.append(pltpu.make_async_copy(groups[g][0], groups[g][1].at[own], loc_sem.at[1 + g]))
    for c in local:
        c.start()

    i = lax.broadcasted_iota(jnp.int32, (length, length), 0)
    s = lax.broadcasted_iota(jnp.int32, (length, length), 1)
    for n, h in enumerate(levels):
        ref = (i & ~(2 * h - 1)) + h - 1
        later = (i & h) != 0
        low = jnp.where(later, ref, i)
        high = jnp.where(later, i, ref)
        sums[n] = jnp.where((s > low) & (s <= high), 1.0, 0.0).astype(bf16)
    sums[len(levels)] = jnp.where(s <= i, 1.0, 0.0).astype(bf16)
    sums[len(levels) + 1] = jnp.where(s > i, 1.0, 0.0).astype(bf16)

    @pl.when(z == 0)
    def _():
        state_in[...] = jnp.zeros_like(state_in)
        kvbuf[:, 0:WINDOW, :] = jnp.zeros((NF, WINDOW, kvbuf.shape[2]), bf16)

    for c in local:
        c.wait()

    def arrive(g):
        for d in range(1, NZ):
            weight_copy(g, d).wait_recv()
            for e in range(1, NT):
                forward_copy(g, d, e).start()
        for d in range(NZ):
            for e in range(1, NT):
                forward_copy(g, d, e).wait_recv()

    def log_sum(n, b):
        m = sums[n]
        return dot(m, fhi[b]) + dot(m, flo[b])

    depth = tok.shape[1]
    arrive(0)
    for d in range(1, NF):
        token_copy(d).wait_recv()

    @pl.loop(0, NF)
    def _(b):
        p = dot(toks[b], W1[...].reshape(depth, -1)).astype(bf16)
        x = p[:, :GLA_KEY].astype(f32) + bias[...]
        forget = (jnp.minimum(x, 0.0) - jnp.log1p(jnp.exp(-jnp.abs(x)))) / tau
        hi = forget.astype(bf16)
        fhi[b] = hi
        flo[b] = (forget - hi.astype(f32)).astype(bf16)
        kkey[b] = p[:, GLA_KEY:2 * GLA_KEY]
        val[b] = p[:, 2 * GLA_KEY:2 * GLA_KEY + GLA_VALUE]
        kvbuf[b, WINDOW:, :] = p[:, 2 * GLA_KEY + GLA_VALUE:]

    def halo_copy():
        return pltpu.make_async_remote_copy(
            src_ref=kvbuf.at[:, pl.ds(length, WINDOW)], dst_ref=kvbuf.at[:, pl.ds(0, WINDOW)],
            send_sem=hsend, recv_sem=hrecv, device_id={"sp": lax.rem(z + 1, NZ)}, device_id_type=MESH)

    def state_copy(b):
        return pltpu.make_async_remote_copy(
            src_ref=state_out.at[b], dst_ref=state_in.at[b],
            send_sem=ssend.at[b], recv_sem=srecv.at[b],
            device_id={"sp": lax.rem(z + 1, NZ)}, device_id_type=MESH)

    @pl.when(z < NZ - 1)
    def _():
        halo_copy().start()

    @pl.loop(0, NF)
    def _(b):
        faded = (kkey[b].astype(f32) * jnp.exp(log_sum(len(levels) + 1, b))).astype(bf16)
        local_state = dot_rows(faded, val[b])
        ones = jnp.ones((length, GLA_VALUE), bf16)
        decay = jnp.exp(dot_rows(fhi[b], ones) + dot_rows(flo[b], ones))

        @pl.when(z > 0)
        def _():
            state_copy(b).wait_recv()

        @pl.when(z < NZ - 1)
        def _():
            state_out[b] = (state_in[b].astype(f32) * decay + local_state).astype(bf16)
            state_copy(b).start()

    arrive(1)

    @pl.when(z > 0)
    def _():
        halo_copy().wait_recv()

    span = length + WINDOW
    row = lax.broadcasted_iota(jnp.int32, (length, span), 0)
    col = lax.broadcasted_iota(jnp.int32, (length, span), 1)
    distance = row - col + WINDOW
    heads = sink.shape[1]
    wq = heads * HEAD_DIM

    @pl.loop(0, NF)
    def _(b):
        p = dot(toks[b], W2[...].reshape(depth, -1)).astype(bf16)
        allowed = (distance >= 0) & (distance < WINDOW) & ((col >= WINDOW) | (z > 0))
        kv = kvbuf[b]
        k, v = kv[:, :HEAD_DIM], kv[:, HEAD_DIM:]
        heads_out = []
        for j in range(heads):
            score = dot_t(p[:, j * HEAD_DIM:(j + 1) * HEAD_DIM], k) * HEAD_DIM ** -0.5
            score = jnp.where(allowed, score, -jnp.inf)
            sk = sink[0:1, j:j + 1]
            top = jnp.maximum(jnp.max(score, axis=1, keepdims=True), sk)
            e = jnp.exp(score - top)
            total = jnp.sum(e, axis=1, keepdims=True) + jnp.exp(sk - top)
            heads_out.append((dot(e.astype(bf16), v) / total).astype(bf16))
        rows[b, :, GLA_VALUE:] = jnp.concatenate(heads_out, axis=1)
        q = p[:, wq:].astype(f32) * GLA_KEY ** -0.5
        k = kkey[b].astype(f32)
        v = val[b]
        ri = lax.broadcasted_iota(jnp.int32, (length, length), 0)
        ci = lax.broadcasted_iota(jnp.int32, (length, length), 1)
        rk = lax.broadcasted_iota(jnp.int32, (length, GLA_KEY), 0)
        scores = jnp.where(ri == ci, dot_t(q.astype(bf16), kkey[b]), 0.0)
        for n, h in enumerate(levels):
            decay = jnp.exp(log_sum(n, b))
            later = (rk & h) != 0
            qh = jnp.where(later, q * decay, 0.0).astype(bf16)
            kh = jnp.where(later, 0.0, k * decay).astype(bf16)
            same = (ri & ~(2 * h - 1)) == (ci & ~(2 * h - 1))
            scores = scores + jnp.where(same, dot_t(qh, kh), 0.0)
        reach = (q * jnp.exp(log_sum(len(levels), b))).astype(bf16)
        oacc[b] = dot(scores.astype(bf16), v) + dot(reach, state_in[b])

    arrive(2)

    def part_copy(d):
        return pltpu.make_async_remote_copy(
            src_ref=part.at[d], dst_ref=rbuf.at[d], send_sem=psend.at[d], recv_sem=precv.at[d],
            device_id={"fs": lax.rem(f + d, NF)}, device_id_type=MESH)

    @pl.loop(1, NF + 1)
    def _(step):
        b = lax.rem(f + step, NF)
        gate = dot(toks[b], W3[...].reshape(depth, -1)).astype(bf16).astype(f32)
        o = oacc[b]
        scaled = o * lax.rsqrt(jnp.mean(o * o, axis=1, keepdims=True) + norm_epsilon)
        rows[b, :, :GLA_VALUE] = (scaled * gain[...] * (gate / (1.0 + jnp.exp(-gate)))).astype(bf16)
        y = dot(rows[b], out_w[...])

        @pl.when(step < NF)
        def _():
            part[step] = y.astype(bf16)
            part_copy(step).start()

        @pl.when(step == NF)
        def _():
            acc = y
            for d in range(1, NF):
                part_copy(d).wait_recv()
                acc = acc + rbuf[d].astype(f32)
            out[...] = acc.astype(bf16)

    for d in range(1, NF):
        token_copy(d).wait_send()
        part_copy(d).wait_send()
    for g in range(3):
        for d in range(1, NZ):
            weight_copy(g, d).wait_send()
        for d in range(NZ):
            for e in range(1, NT):
                forward_copy(g, d, e).wait_send()

    @pl.when(z < NZ - 1)
    def _():
        halo_copy().wait_send()
        for b in range(NF):
            state_copy(b).wait_send()


def shards(
    NZ, NF, NT,
    tokens, linear_query, linear_key, linear_decay, linear_value, linear_gate, decay_bias,
    norm_gain, window_query, window_key, window_value, sink_logit, linear_output, window_output,
):
    _, length, depth = tokens.shape
    w1 = jnp.concatenate([linear_decay, linear_key, linear_value, window_key, window_value], axis=1)
    w2 = jnp.concatenate([window_query, linear_query], axis=1)
    w3 = linear_gate
    out_w = jnp.concatenate([linear_output, window_output], axis=0)
    kb = w1.shape[0]
    n = NZ * NT
    levels = []
    h = 1
    while h < length:
        levels.append(h)
        h *= 2
    vm = pltpu.VMEM
    dma = pltpu.SemaphoreType.DMA
    kv_width = window_key.shape[1] + window_value.shape[1]
    out_rows = out_w.shape[0]
    result = pl.pallas_call(
        functools.partial(kernel, NZ, NF, NT, tuple(levels)),
        out_shape=jax.ShapeDtypeStruct((length, depth), bf16),
        in_specs=[pl.BlockSpec(memory_space=vm)] * 8,
        out_specs=pl.BlockSpec(memory_space=vm),
        scratch_shapes=[
            vm((NF, length, depth), bf16),
            vm((n, kb, w1.shape[1]), bf16),
            vm((n, kb, w2.shape[1]), bf16),
            vm((n, kb, w3.shape[1]), bf16),
            vm((len(levels) + 2, length, length), bf16),
            vm((NF, length, GLA_KEY), bf16),
            vm((NF, length, GLA_KEY), bf16),
            vm((NF, length, GLA_KEY), bf16),
            vm((NF, length, GLA_VALUE), bf16),
            vm((NF, length + WINDOW, kv_width), bf16),
            vm((8, 128), f32),
            vm((NF, length, GLA_VALUE), f32),
            vm((NF, GLA_KEY, GLA_VALUE), bf16),
            vm((NF, GLA_KEY, GLA_VALUE), bf16),
            vm((NF, length, out_rows), bf16),
            vm((NF, length, depth), bf16),
            vm((NF, length, depth), bf16),
            dma((4,)),
            dma((3, NZ)), dma((3, NZ)),
            dma((3, NZ, NT)), dma((3, NZ, NT)),
            dma((NF,)), dma((NF,)),
            dma((NF,)), dma((NF,)),
            dma, dma,
            dma((NF,)), dma((NF,)),
        ],
        compiler_params=pltpu.CompilerParams(
            collective_id=0, has_side_effects=True, vmem_limit_bytes=60 * 1024 * 1024),
        name="layer",
    )(tokens[0], w1, w2, w3, decay_bias[None], norm_gain[None], sink_logit[None], out_w)
    return result[None]


def solution(mesh):
    shape = mesh.shape
    return jax.shard_map(
        functools.partial(shards, shape["sp"], shape["fs"], shape["tp"]),
        mesh=mesh,
        in_specs=(
            P(("fs", "tp"), "sp", None),
            P(("sp", "tp"), "fs"),
            P(("sp", "tp"), "fs"),
            P(("sp", "tp"), "fs"),
            P(("sp", "tp"), "fs"),
            P(("sp", "tp"), "fs"),
            P("fs"),
            P(),
            P(("sp", "tp"), "fs"),
            P(("sp", "tp"), "fs"),
            P(("sp", "tp"), "fs"),
            P("fs"),
            P("fs", None),
            P("fs", None),
        ),
        out_specs=P(("fs", "tp"), "sp", None),
        check_vma=False,
    )
```

profile of v0, /device:TPU:248, one launch (start us, length us, event | category | flops | bytes accessed | tf_op | source)
XLA Modules:
  0.0 242.7 jit_solution(6178069351674519949)
XLA Ops:
  0.0 1.3 pad_maximum_fusion.1.w2
  1.3 1.5 concatenate.9.w1
  2.8 3.1 %pad_maximum_fusion.out_w = bf16[512,2048]{1,0:T(8,128)(2,1)} fusion(bf16[256,2048]{1,0:T(8,128)(2,1)} %param.27, bf16[256,2048]{1,0:T(8,128)(2,1)} %param.26), kind=kLoop, calls=%fused_computation | loop fusion | flops 4194304 | bytes 4194304 | tf_op jit(solution)/shard_map/concatenate | solution.py:269
  5.9 234.6 %layer.1 = bf16[192,2048]{1,0:T(8,128)(2,1)} custom-call(bf16[192,2048]{1,0:T(8,128)(2,1)} %bitcast.6, bf16[32,640]{1,0:T(8,128)(2,1)} %concatenate.9.w1, bf16[32,384]{1,0:T(8,128)(2,1)} %pad_maximum_fusion.1.w2, bf16[32,256]{1,0:T(8,128)(2,1)} %w3.1, f32[1,128]{1,0:T(1,128)} %bitcast.8, f32[1,256]{1,0:T(1,128)} %bitcast.7, f32[1,4]{1,0:T(1,128)} %bitcast.9, ...), custom_call_target="tpu_custom_call" | custom-call | tf_op jit(solution)/shard_map/layer/pallas_call | solution.py:281
  240.6 2.1 copy.16
where the time goes:
time: 243 us
  Pallas kernels  235 us (97%)
  other arithmetic  4.48 us (2%)
  local copies, waits for them, and re-layouts  3.56 us (1%)
    pallas_call x1, Pallas kernels, shards(): pl.pallas_call(functools.partial(kernel, NZ, NF, NT, tuple(levels)), out_...  235 us

commit v1 on v0

v1 whole, which is shorter than its diff:
```python
import functools

import jax
import jax.numpy as jnp
from jax import lax
from jax.experimental import pallas as pl
from jax.experimental.pallas import tpu as pltpu
from jax.sharding import PartitionSpec as P

GLA_KEY = 128
GLA_VALUE = 256
HEAD_DIM = 64
WINDOW = 128
NY = 4

norm_epsilon = 1e-05
MESH = pl.DeviceIdType.MESH
f32, bf16 = jnp.float32, jnp.bfloat16


def dot(a, b):
    return jnp.dot(a, b, preferred_element_type=f32)


def dot_t(a, b):
    return lax.dot_general(a, b, (((1,), (1,)), ((), ())), preferred_element_type=f32)


def dot_rows(a, b):
    return lax.dot_general(a, b, (((0,), (0,)), ((), ())), preferred_element_type=f32)


def kernel(
    NS, NF, NT, levels,
    tok, w_decay, w_key, w_value, w_wq, w_lq, w_gate, lin_o, win_o, w_wk, w_wv, bias, gain, sink,
    out,
    toks, W1, W2, out_w, sums, f2, kkey, val, kvbuf, lst, arr, pre, state_in, rows, oacc, reach, gates, part, rbuf,
    lsem, zs, zr, ys, yr, rs, rr, dsnd, drcv, ts, tr, hs, hr, asnd, arcv, qs, qr, ps, pr,
):
    sp, f, t = lax.axis_index("sp"), lax.axis_index("fs"), lax.axis_index("tp")
    NZ = NS // NY
    zz, yy = sp // NY, lax.rem(sp, NY)
    length, depth = tok.shape
    half = length // 2
    tau = NS * length // 16
    LK = GLA_KEY
    RP = LK // NZ
    groups = (W1, W2)

    def at_z(d):
        return {"sp": lax.rem(zz + d, NZ) * NY + yy}

    def at_y(d):
        return {"sp": zz * NY + lax.rem(yy + d, NY)}

    def at_f(d):
        return {"fs": lax.rem(f + d, NF)}

    other = {"tp": 1 - t}

    def rc(src, dst, ssem, rsem, dev):
        return pltpu.make_async_remote_copy(
            src_ref=src, dst_ref=dst, send_sem=ssem, recv_sem=rsem, device_id=dev, device_id_type=MESH)

    barrier = pltpu.get_barrier_semaphore()
    greet = [at_z(d) for d in range(1, NZ)] + [at_y(1), at_y(NY - 1)] + [at_f(d) for d in range(1, NF)] + [other]
    for dev in greet:
        pl.semaphore_signal(barrier, inc=1, device_id=dev, device_id_type=MESH)
    own1, own2 = W1.at[zz, yy, t], W2.at[zz, yy, t]
    loads = [
        (tok, toks.at[f]),
        (w_decay, own1.at[:, 0:128]), (w_key, own1.at[:, 128:256]), (w_value, own1.at[:, 256:512]),
        (w_wq, own2.at[:, 0:256]), (w_lq, own2.at[:, 256:384]), (w_gate, own2.at[:, 384:640]),
        (lin_o, out_w.at[0:256]), (win_o, out_w.at[256:512]),
    ]
    local = [pltpu.make_async_copy(a, b, lsem.at[n]) for n, (a, b) in enumerate(loads)]
    for c in local:
        c.start()
    W1[zz, yy, t, :, 512:640] = jnp.concatenate([w_wk[...], w_wv[...]], axis=1)

    i0 = lax.broadcasted_iota(jnp.int32, (length, length), 0)
    s0 = lax.broadcasted_iota(jnp.int32, (length, length), 1)
    for n, h in enumerate(levels):
        ref = (i0 & ~(2 * h - 1)) + h - 1
        later = (i0 & h) != 0
        low = jnp.where(later, ref, i0)
        high = jnp.where(later, i0, ref)
        sums[n] = jnp.where((s0 > low) & (s0 <= high), 1.0, 0.0).astype(bf16)
    sums[len(levels)] = jnp.where(s0 <= i0, 1.0, 0.0).astype(bf16)
    sums[len(levels) + 1] = jnp.where(s0 > i0, 1.0, 0.0).astype(bf16)

    @pl.when(sp == 0)
    def _():
        kvbuf[:, 0:WINDOW, :] = jnp.zeros((NF, WINDOW, kvbuf.shape[2]), bf16)

    for c in local[:7]:
        c.wait()
    pl.semaphore_wait(barrier, len(greet))

    def token_copy(j):
        to_right = j in (0, 2, 4)
        first = j in (0, 3, 4)
        who = f if j < 4 else lax.rem(f + (NF - 1 if to_right else 1), NF)
        ref = toks.at[who, pl.ds(0 if first else half, half)]
        return rc(ref, ref, ts.at[j], tr.at[j], at_f(1 if to_right else NF - 1))

    def slot(g, k, yo):
        return groups[g].at[lax.rem(zz - k + NZ, NZ), lax.rem(yy - yo + NY, NY), t]

    def z_copy(g, d):
        ref = slot(g, 0, 0)
        return rc(ref, ref, zs.at[g, d], zr.at[g, d], at_z(d))

    def y_copy(g, k, side):
        ref = slot(g, k, 0)
        return rc(ref, ref, ys.at[g, side, k], yr.at[g, side, k], at_y(1 if side == 0 else NY - 1))

    def relay_copy(g, k):
        up = k % 2 == 0
        ref = slot(g, k, 1 if up else NY - 1)
        return rc(ref, ref, rs.at[g, k], rr.at[g, k], at_y(1 if up else NY - 1))

    def core_copy(g, k, yo):
        ref = slot(g, k, yo)
        return rc(ref, ref, dsnd.at[g], drcv.at[g], other)

    def core_all(g):
        ref = groups[g].at[:, :, t]
        return rc(ref, ref, dsnd.at[g], drcv.at[g], other)

    zorder = []
    for d in range(1, NZ // 2 + 1):
        zorder += [d] if 2 * d == NZ else [d, NZ - d]

    def pass_y(g, k):
        y_copy(g, k, 0).start()
        y_copy(g, k, 1).start()
        core_copy(g, k, 0).start()

    def z_arrive(g):
        for k in zorder:
            z_copy(g, k).wait_recv()
            pass_y(g, k)

    def y_arrive(g):
        for k in [0] + zorder:
            y_copy(g, k, 0).wait_recv()
            if k % 2 == 0:
                relay_copy(g, k).start()
            core_copy(g, k, 1).start()
            y_copy(g, k, 1).wait_recv()
            if k % 2 == 1:
                relay_copy(g, k).start()
            core_copy(g, k, NY - 1).start()

    def relay_arrive(g):
        for k in [0] + zorder:
            relay_copy(g, k).wait_recv()
            core_copy(g, k, 2).start()

    for d in zorder:
        z_copy(0, d).start()
    for j in range(2):
        token_copy(j).start()
    pass_y(0, 0)
    for j in range(2, 4):
        token_copy(j).start()
    for d in zorder:
        z_copy(1, d).start()
    z_arrive(0)
    token_copy(0).wait_recv()
    token_copy(4).start()
    token_copy(1).wait_recv()
    token_copy(5).start()
    y_arrive(0)
    pass_y(1, 0)
    relay_arrive(0)
    core_all(0).wait_recv()

    def order(i):
        return lax.rem(f + jnp.where(i == 0, 0, jnp.where(i == 1, NF - 1, i - 1)), NF)

    def log_sum(n, b):
        x = dot(sums[n], f2[b])
        return x[:, :LK] + x[:, LK:]

    def halo_copy(b):
        return rc(kvbuf.at[b, pl.ds(length, WINDOW)], kvbuf.at[b, pl.ds(0, WINDOW)], hs.at[b], hr.at[b],
                  {"sp": lax.rem(sp + 1, NS)})

    def piece_copy(b, r, src_sp):
        return rc(lst.at[b, r], arr.at[src_sp], asnd.at[b, r], arcv.at[src_sp], {"sp": r * NY + b})

    lane = lax.broadcasted_iota(jnp.int32, (LK, 128), 1)

    @pl.loop(0, NF)
    def _(i):
        b = order(i)

        @pl.when(i == 1)
        def _():
            z_arrive(1)
            token_copy(2).wait_recv()

        @pl.when(i == 2)
        def _():
            y_arrive(1)
            token_copy(3).wait_recv()

        @pl.when(i == 3)
        def _():
            relay_arrive(1)
            token_copy(4).wait_recv()
            token_copy(5).wait_recv()

        p = dot(toks[b], W1[...].reshape(depth, -1)).astype(bf16)
        x = p[:, :LK].astype(f32) + bias[...]
        forget = (jnp.minimum(x, 0.0) - jnp.log1p(jnp.exp(-jnp.abs(x)))) / tau
        hi = forget.astype(bf16)
        f2[b] = jnp.concatenate([hi, (forget - hi.astype(f32)).astype(bf16)], axis=1)
        k = p[:, LK:2 * LK]
        v = p[:, 2 * LK:2 * LK + GLA_VALUE]
        kkey[b] = k
        val[b] = v
        kvbuf[b, WINDOW:, :] = p[:, 2 * LK + GLA_VALUE:]
        faded = (k.astype(f32) * jnp.exp(log_sum(len(levels) + 1, b))).astype(bf16)
        state = dot_rows(faded, v).astype(bf16)
        total = dot_rows(f2[b], jnp.ones((length, 128), bf16))
        decay = jnp.exp(total[:LK] + total[LK:])
        dhi = decay.astype(bf16)
        dlo = (decay - dhi.astype(f32)).astype(bf16)
        packed = jnp.where(lane < 64, dhi.astype(f32), dlo.astype(f32)).astype(bf16)
        lst[b] = jnp.concatenate([state, packed], axis=1).reshape(NZ, RP, GLA_VALUE + 128)

        @pl.when(sp < NS - 1)
        def _():
            halo_copy(b).start()

        @pl.loop(0, NZ)
        def _(r):
            @pl.when(r * NY + b != sp)
            def _():
                piece_copy(b, r, sp).start()

            @pl.when(r * NY + b == sp)
            def _():
                arr[sp] = lst[b, r]

    core_all(1).wait_recv()

    def prefix_copy(s):
        return rc(pre.at[s], state_in.at[yy, zz], qs.at[s], qr.at[sp], {"sp": s})

    def scan():
        def step(s, carry):
            @pl.when(s != sp)
            def _():
                piece_copy(0, 0, s).wait_recv()

            pre[s] = carry.astype(bf16)
            x = arr[s].astype(f32)
            g = x[:, GLA_VALUE:]
            g = g + pltpu.roll(g, 64, 1)
            return carry * jnp.concatenate([g, g], axis=1) + x[:, :GLA_VALUE]

        lax.fori_loop(0, NS, step, jnp.zeros((RP, GLA_VALUE), f32))

        @pl.loop(0, NS)
        def _(s):
            @pl.when(s != sp)
            def _():
                prefix_copy(s).start()

            @pl.when(s == sp)
            def _():
                state_in[yy, zz] = pre[s]

    span = length + WINDOW
    row = lax.broadcasted_iota(jnp.int32, (length, span), 0)
    col = lax.broadcasted_iota(jnp.int32, (length, span), 1)
    distance = row - col + WINDOW
    heads = sink.shape[1]
    wq = heads * HEAD_DIM

    @pl.loop(0, NF)
    def _(i):
        b = order(i)

        @pl.when(i == 2)
        def _():
            scan()

        @pl.when(sp > 0)
        def _():
            halo_copy(b).wait_recv()

        p = dot(toks[b], W2[...].reshape(depth, -1)).astype(bf16)
        allowed = (distance >= 0) & (distance < WINDOW) & ((col >= WINDOW) | (sp > 0))
        kv = kvbuf[b]
        k, v = kv[:, :HEAD_DIM], kv[:, HEAD_DIM:]
        heads_out = []
        for j in range(heads):
            score = dot_t(p[:, j * HEAD_DIM:(j + 1) * HEAD_DIM], k) * HEAD_DIM ** -0.5
            score = jnp.where(allowed, score, -jnp.inf)
            sk = sink[0:1, j:j + 1]
            top = jnp.maximum(jnp.max(score, axis=1, keepdims=True), sk)
            e = jnp.exp(score - top)
            total = jnp.sum(e, axis=1, keepdims=True) + jnp.exp(sk - top)
            heads_out.append((dot(e.astype(bf16), v) / total).astype(bf16))
        rows[b, :, GLA_VALUE:] = jnp.concatenate(heads_out, axis=1)
        gates[b] = p[:, wq + LK:]
        q = p[:, wq:wq + LK].astype(f32) * LK ** -0.5
        k = kkey[b].astype(f32)
        ri = lax.broadcasted_iota(jnp.int32, (length, length), 0)
        ci = lax.broadcasted_iota(jnp.int32, (length, length), 1)
        rk = lax.broadcasted_iota(jnp.int32, (length, LK), 0)
        scores = jnp.where(ri == ci, dot_t(q.astype(bf16), kkey[b]), 0.0)
        for n, h in enumerate(levels):
            decay = jnp.exp(log_sum(n, b))
            later = (rk & h) != 0
            qh = jnp.where(later, q * decay, 0.0).astype(bf16)
            kh = jnp.where(later, 0.0, k * decay).astype(bf16)
            same = (ri & ~(2 * h - 1)) == (ci & ~(2 * h - 1))
            scores = scores + jnp.where(same, dot_t(qh, kh), 0.0)
        reach[b] = (q * jnp.exp(log_sum(len(levels), b))).astype(bf16)
        oacc[b] = dot(scores.astype(bf16), val[b])

    for c in local[7:]:
        c.wait()

    def part_copy(d):
        return rc(part.at[d], rbuf.at[d], ps.at[d], pr.at[d], at_f(d))

    @pl.loop(1, NF + 1)
    def _(step):
        b = lax.rem(f + step, NF)

        @pl.loop(0, NZ)
        def _(r):
            o = r * NY + b

            @pl.when(o != sp)
            def _():
                rc(pre.at[0], state_in.at[b, r], qs.at[0], qr.at[o], {"sp": o}).wait_recv()

        gate = gates[b].astype(f32)
        o = oacc[b] + dot(reach[b], state_in[b].reshape(LK, GLA_VALUE))
        scaled = o * lax.rsqrt(jnp.mean(o * o, axis=1, keepdims=True) + norm_epsilon)
        rows[b, :, :GLA_VALUE] = (scaled * gain[...] * (gate / (1.0 + jnp.exp(-gate)))).astype(bf16)
        y = dot(rows[b], out_w[...])

        @pl.when(step < NF)
        def _():
            part[step] = y.astype(bf16)
            part_copy(step).start()

        @pl.when(step == NF)
        def _():
            acc = y
            for d in range(1, NF):
                part_copy(d).wait_recv()
                acc = acc + rbuf[d].astype(f32)
            out[...] = acc.astype(bf16)

    for j in range(6):
        token_copy(j).wait_send()
    for d in range(1, NF):
        part_copy(d).wait_send()
    for g in range(2):
        for d in range(1, NZ):
            z_copy(g, d).wait_send()
        for k in range(NZ):
            y_copy(g, k, 0).wait_send()
            y_copy(g, k, 1).wait_send()
            relay_copy(g, k).wait_send()
        core_all(g).wait_send()

    @pl.when(sp < NS - 1)
    def _():
        for b in range(NF):
            halo_copy(b).wait_send()

    @pl.loop(0, NS)
    def _(s):
        @pl.when(s != sp)
        def _():
            piece_copy(lax.rem(s, NY), s // NY, sp).wait_send()
            prefix_copy(s).wait_send()


def shards(
    NS, NF, NT,
    tokens, linear_query, linear_key, linear_decay, linear_value, linear_gate, decay_bias,
    norm_gain, window_query, window_key, window_value, sink_logit, linear_output, window_output,
):
    _, length, depth = tokens.shape
    kb = linear_query.shape[0]
    NZ = NS // NY
    levels = []
    h = 1
    while h < length:
        levels.append(h)
        h *= 2
    vm = pltpu.VMEM
    dma = pltpu.SemaphoreType.DMA
    kv_width = window_key.shape[1] + window_value.shape[1]
    out_rows = linear_output.shape[0] + window_output.shape[0]
    width1 = 2 * GLA_KEY + GLA_VALUE + kv_width
    width2 = window_query.shape[1] + GLA_KEY + GLA_VALUE
    anyspec = pl.BlockSpec(memory_space=pl.ANY)
    vspec = pl.BlockSpec(memory_space=vm)
    result = pl.pallas_call(
        functools.partial(kernel, NS, NF, NT, tuple(levels)),
        out_shape=jax.ShapeDtypeStruct((length, depth), bf16),
        in_specs=[anyspec] * 9 + [vspec] * 5,
        out_specs=vspec,
        scratch_shapes=[
            vm((NF, length, depth), bf16),
            vm((NZ, NY, NT, kb, width1), bf16),
            vm((NZ, NY, NT, kb, width2), bf16),
            vm((out_rows, depth), bf16),
            vm((len(levels) + 2, length, length), bf16),
            vm((NF, length, 2 * GLA_KEY), bf16),
            vm((NF, length, GLA_KEY), bf16),
            vm((NF, length, GLA_VALUE), bf16),
            vm((NF, length + WINDOW, kv_width), bf16),
            vm((NF, NZ, GLA_KEY // NZ, GLA_VALUE + 128), bf16),
            vm((NS, GLA_KEY // NZ, GLA_VALUE + 128), bf16),
            vm((NS, GLA_KEY // NZ, GLA_VALUE), bf16),
            vm((NF, NZ, GLA_KEY // NZ, GLA_VALUE), bf16),
            vm((NF, length, out_rows), bf16),
            vm((NF, length, GLA_VALUE), f32),
            vm((NF, length, GLA_KEY), bf16),
            vm((NF, length, GLA_VALUE), bf16),
            vm((NF, length, depth), bf16),
            vm((NF, length, depth), bf16),
            dma((9,)),
            dma((2, NZ)), dma((2, NZ)),
            dma((2, 2, NZ)), dma((2, 2, NZ)),
            dma((2, NZ)), dma((2, NZ)),
            dma((2,)), dma((2,)),
            dma((6,)), dma((6,)),
            dma((NF,)), dma((NF,)),
            dma((NF, NZ)), dma((NS,)),
            dma((NS,)), dma((NS,)),
            dma((NF,)), dma((NF,)),
        ],
        compiler_params=pltpu.CompilerParams(
            collective_id=0, has_side_effects=True, vmem_limit_bytes=60 * 1024 * 1024),
        name="layer",
    )(tokens[0], linear_decay, linear_key, linear_value, window_query, linear_query, linear_gate,
      linear_output, window_output, window_key, window_value,
      decay_bias[None], norm_gain[None], sink_logit[None])
    return result[None]


def solution(mesh):
    shape = mesh.shape
    return jax.shard_map(
        functools.partial(shards, shape["sp"], shape["fs"], shape["tp"]),
        mesh=mesh,
        in_specs=(
            P(("fs", "tp"), "sp", None),
            P(("sp", "tp"), "fs"),
            P(("sp", "tp"), "fs"),
            P(("sp", "tp"), "fs"),
            P(("sp", "tp"), "fs"),
            P(("sp", "tp"), "fs"),
            P("fs"),
            P(),
            P(("sp", "tp"), "fs"),
            P(("sp", "tp"), "fs"),
            P(("sp", "tp"), "fs"),
            P("fs"),
            P("fs", None),
            P("fs", None),
        ),
        out_specs=P(("fs", "tp"), "sp", None),
        check_vma=False,
    )
```

time: 243 us -> 107 us (0.44)
  the two profiles are of different devices: /device:TPU:248 before, /device:TPU:1 now
where the time goes in v1:
time: 107 us; the launch traced here: 105 us
  Pallas kernels  103 us (96%)
  local copies, waits for them, and re-layouts  2.09 us (2%)
    pallas_call x1, Pallas kernels, shards(): pl.pallas_call(functools.partial(kernel, NS, NF, NT, tuple(levels)), out_...  103 us

profile of v1, /device:TPU:1, one launch (start us, length us, event | category | flops | bytes accessed | tf_op | source)
XLA Modules:
  0.0 105.0 jit_solution(777513239102779163)
XLA Ops:
  0.0 102.9 %layer.1 = bf16[192,2048]{1,0:T(8,128)(2,1)} custom-call(bf16[192,2048]{1,0:T(8,128)(2,1)} %bitcast.6, bf16[32,128]{1,0:T(8,128)(2,1)} %w_decay.1, bf16[32,128]{1,0:T(8,128)(2,1)} %w_key.1, bf16[32,256]{1,0:T(8,128)(2,1)} %w_value.1, bf16[32,256]{1,0:T(8,128)(2,1)} %w_wq.1, bf16[32,128]{1,0:T(8,128)(2,1)} %w_lq.1, bf16[32,256]{1,0:T(8,128)(2,1)} %w_gate.1, ...), custom_call_target="tpu_custom_call" | custom-call | tf_op jit(solution)/shard_map/layer/pallas_call | solution.py:412
  102.9 2.1 %copy.16 = bf16[1,192,2048]{2,1,0:T(8,128)(2,1)} copy(bf16[1,192,2048]{2,1,0:T(8,128)(2,1)} %bitcast.5) | data formatting | bytes 1572864

commit v2 on v1

v2 whole, which is shorter than its diff:
```python
import functools

import jax
import jax.numpy as jnp
from jax import lax
from jax.experimental import pallas as pl
from jax.experimental.pallas import tpu as pltpu
from jax.sharding import PartitionSpec as P

GLA_KEY = 128
GLA_VALUE = 256
HEAD_DIM = 64
WINDOW = 128
NY = 4

norm_epsilon = 1e-05
MESH = pl.DeviceIdType.MESH
f32, bf16 = jnp.float32, jnp.bfloat16


def dot(a, b):
    return jnp.dot(a, b, preferred_element_type=f32)


def dot_t(a, b):
    return lax.dot_general(a, b, (((1,), (1,)), ((), ())), preferred_element_type=f32)


def dot_rows(a, b):
    return lax.dot_general(a, b, (((0,), (0,)), ((), ())), preferred_element_type=f32)


def kernel(
    NS, NF, NT, levels,
    tok, w_decay, w_key, w_value, w_lq, w_wq, w_gate, lin_o, win_o, w_wk, w_wv, bias, gain, sink,
    out,
    toks, W1, W2, OW, sums, f2, kkey, val, query, kvbuf, lst, arr, pre, state_in,
    lrow, wrow, lall, wall, oacc, reach, gates, acc,
    lsem, zs, zr, ys, yr, rs, rr, dsnd, drcv, ts, tr, hs, hr, asnd, arcv, qs, qr,
    ls, lr, ws, wr, xs, xr, os, orr,
):
    sp, f, t = lax.axis_index("sp"), lax.axis_index("fs"), lax.axis_index("tp")
    NZ = NS // NY
    zz, yy = sp // NY, lax.rem(sp, NY)
    length, depth = tok.shape
    half = length // 2
    tau = NS * length // 16
    LK = GLA_KEY
    RP = LK // NZ
    groups = (W1, W2)
    scope = jax.named_scope

    def at_z(d):
        return {"sp": lax.rem(zz + d, NZ) * NY + yy}

    def at_y(d):
        return {"sp": zz * NY + lax.rem(yy + d, NY)}

    def at_f(d):
        return {"fs": lax.rem(f + d, NF)}

    other = {"tp": 1 - t}

    def rc(src, dst, ssem, rsem, dev):
        return pltpu.make_async_remote_copy(
            src_ref=src, dst_ref=dst, send_sem=ssem, recv_sem=rsem, device_id=dev, device_id_type=MESH)

    barrier = pltpu.get_barrier_semaphore()
    greet = [at_z(d) for d in range(1, NZ)] + [at_y(1), at_y(NY - 1)] + [at_f(d) for d in range(1, NF)] + [other]
    for dev in greet:
        pl.semaphore_signal(barrier, inc=1, device_id=dev, device_id_type=MESH)
    own1, own2 = W1.at[zz, yy, t], W2.at[zz, yy, t]
    loads = [
        (tok, toks.at[f]),
        (w_decay, own1.at[:, 0:128]), (w_key, own1.at[:, 128:256]), (w_value, own1.at[:, 256:512]),
        (w_lq, own1.at[:, 512:640]),
        (w_wq, own2.at[:, 0:256]), (w_gate, own2.at[:, 256:512]),
        (lin_o, OW.at[0]), (win_o, OW.at[NF]),
    ]
    local = [pltpu.make_async_copy(a, b, lsem.at[n]) for n, (a, b) in enumerate(loads)]
    for c in local:
        c.start()
    W1[zz, yy, t, :, 640:768] = jnp.concatenate([w_wk[...], w_wv[...]], axis=1)

    i0 = lax.broadcasted_iota(jnp.int32, (length, length), 0)
    s0 = lax.broadcasted_iota(jnp.int32, (length, length), 1)
    for n, h in enumerate(levels):
        ref = (i0 & ~(2 * h - 1)) + h - 1
        later = (i0 & h) != 0
        low = jnp.where(later, ref, i0)
        high = jnp.where(later, i0, ref)
        sums[n] = jnp.where((s0 > low) & (s0 <= high), 1.0, 0.0).astype(bf16)
    sums[len(levels)] = jnp.where(s0 <= i0, 1.0, 0.0).astype(bf16)
    sums[len(levels) + 1] = jnp.where(s0 > i0, 1.0, 0.0).astype(bf16)

    @pl.when(sp == 0)
    def _():
        kvbuf[:, 0:WINDOW, :] = jnp.zeros((NF, WINDOW, kvbuf.shape[2]), bf16)

    with scope("a_loads"):
        for c in local[:7]:
            c.wait()
    with scope("b_barrier"):
        pl.semaphore_wait(barrier, len(greet))

    def x_step(j):
        return j in (0, 2, 4), j in (0, 3, 4)

    def token_copy(j):
        right, first = x_step(j)
        who = f if j < 4 else lax.rem(f + (NF - 1 if right else 1), NF)
        ref = toks.at[who, pl.ds(0 if first else half, half)]
        return rc(ref, ref, ts.at[j], tr.at[j], at_f(1 if right else NF - 1))

    orows = OW.shape[1]
    ocols = depth // NT
    cols_t = pl.ds(pl.multiple_of(t * ocols, ocols), ocols)

    def ow_part(rel, first):
        return OW.at[NF + rel, pl.ds(0 if first else orows // 2, orows // 2), cols_t]

    def ow_copy(j):
        right, first = x_step(j)
        src = 0 if j < 4 else (NF - 1 if right else 1)
        dst = (src + (NF - 1 if right else 1)) % NF
        return rc(ow_part(src, first), ow_part(dst, first), os.at[j], orr.at[j], at_f(1 if right else NF - 1))

    def ow_core(j):
        right, first = x_step(j)
        ref = ow_part((NF - 1 if right else 1) if j < 4 else 2, first)
        return rc(ref, ref, dsnd.at[3], drcv.at[3], other)

    def ow_core_all():
        ref = OW.at[pl.ds(NF + 1, NF - 1), :, cols_t]
        return rc(ref, ref, dsnd.at[3], drcv.at[3], other)

    tile_r = orows // (NS // 2)
    tile_c = ocols // 2

    def ow_tile(k, yo):
        z1, y1 = lax.rem(zz - k + NZ, NZ), lax.rem(yy - yo + NY, NY)
        s1 = z1 * NY + y1
        return (pl.ds(pl.multiple_of((s1 // 2) * tile_r, tile_r), tile_r),
                pl.ds(pl.multiple_of((t * 2 + lax.rem(s1, 2)) * tile_c, tile_c), tile_c))

    def slice_copy(d):
        r, c = ow_tile(0, 0)
        return rc(OW.at[0, r, c], OW.at[NF - d, r, c], xs.at[d], xr.at[d], at_f(d))

    def slot(g, k, yo):
        if g == 2:
            r, c = ow_tile(k, yo)
            return OW.at[pl.ds(1, NF - 1), r, c]
        return groups[g].at[lax.rem(zz - k + NZ, NZ), lax.rem(yy - yo + NY, NY), t]

    def z_copy(g, d):
        ref = slot(g, 0, 0)
        return rc(ref, ref, zs.at[g, d], zr.at[g, d], at_z(d))

    def y_copy(g, k, side):
        ref = slot(g, k, 0)
        return rc(ref, ref, ys.at[g, side, k], yr.at[g, side, k], at_y(1 if side == 0 else NY - 1))

    def relay_copy(g, k):
        up = k % 2 == 0
        ref = slot(g, k, 1 if up else NY - 1)
        return rc(ref, ref, rs.at[g, k], rr.at[g, k], at_y(1 if up else NY - 1))

    def core_copy(g, k, yo):
        ref = slot(g, k, yo)
        return rc(ref, ref, dsnd.at[g], drcv.at[g], other)

    def core_all(g):
        ref = OW.at[pl.ds(1, NF - 1), :, cols_t] if g == 2 else groups[g].at[:, :, t]
        return rc(ref, ref, dsnd.at[g], drcv.at[g], other)

    zorder = []
    for d in range(1, NZ // 2 + 1):
        zorder += [d] if 2 * d == NZ else [d, NZ - d]

    def z_send(g):
        for d in zorder:
            z_copy(g, d).start()

    def pass_y(g, k):
        y_copy(g, k, 0).start()
        y_copy(g, k, 1).start()
        core_copy(g, k, 0).start()

    def z_arrive(g):
        for k in zorder:
            z_copy(g, k).wait_recv()
            pass_y(g, k)

    def y_arrive(g):
        for k in [0] + zorder:
            y_copy(g, k, 0).wait_recv()
            if k % 2 == 0:
                relay_copy(g, k).start()
            core_copy(g, k, 1).start()
            y_copy(g, k, 1).wait_recv()
            if k % 2 == 1:
                relay_copy(g, k).start()
            core_copy(g, k, NY - 1).start()

    def relay_arrive(g):
        for k in [0] + zorder:
            relay_copy(g, k).wait_recv()
            core_copy(g, k, 2).start()

    z_send(0)
    for j in range(2):
        token_copy(j).start()
    pass_y(0, 0)
    for j in range(2, 4):
        token_copy(j).start()
    z_send(1)
    with scope("c_z0"):
        z_arrive(0)
    with scope("d_tokfwd"):
        for j in range(2):
            token_copy(j).wait_recv()
            token_copy(4 + j).start()
    for c in local[7:]:
        c.wait()
    for d in range(1, NF):
        slice_copy(d).start()
    for j in range(4):
        ow_copy(j).start()
    with scope("e_y0"):
        y_arrive(0)
    pass_y(1, 0)
    with scope("e_z1"):
        z_arrive(1)
    with scope("f_relay0"):
        relay_arrive(0)
    with scope("g_core0"):
        core_all(0).wait_recv()

    def order(i):
        return lax.rem(f + jnp.where(i == 0, 0, jnp.where(i == 1, NF - 1, i - 1)), NF)

    def log_sum(n, b):
        x = dot(sums[n], f2[b])
        return x[:, :LK] + x[:, LK:]

    def halo_copy(b):
        return rc(kvbuf.at[b, pl.ds(length, WINDOW)], kvbuf.at[b, pl.ds(0, WINDOW)], hs.at[b], hr.at[b],
                  {"sp": lax.rem(sp + 1, NS)})

    def piece_copy(b, r, src_sp):
        return rc(lst.at[b, r], arr.at[src_sp], asnd.at[b, r], arcv.at[src_sp], {"sp": r * NY + b})

    lane = lax.broadcasted_iota(jnp.int32, (LK, 128), 1)

    @pl.loop(0, NF)
    def _(i):
        b = order(i)

        @pl.when(i == 1)
        def _():
            with scope("h_tok1"):
                token_copy(2).wait_recv()

        @pl.when(i == 2)
        def _():
            with scope("h_tok2"):
                token_copy(3).wait_recv()

        @pl.when(i == 3)
        def _():
            with scope("h_tok3"):
                token_copy(4).wait_recv()
                token_copy(5).wait_recv()

        p = dot(toks[b], W1[...].reshape(depth, -1)).astype(bf16)
        x = p[:, :LK].astype(f32) + bias[...]
        forget = (jnp.minimum(x, 0.0) - jnp.log1p(jnp.exp(-jnp.abs(x)))) / tau
        hi = forget.astype(bf16)
        f2[b] = jnp.concatenate([hi, (forget - hi.astype(f32)).astype(bf16)], axis=1)
        k = p[:, LK:2 * LK]
        v = p[:, 2 * LK:2 * LK + GLA_VALUE]
        kkey[b] = k
        val[b] = v
        query[b] = p[:, 512:640]
        kvbuf[b, WINDOW:, :] = p[:, 640:]
        faded = (k.astype(f32) * jnp.exp(log_sum(len(levels) + 1, b))).astype(bf16)
        state = dot_rows(faded, v).astype(bf16)
        total = dot_rows(f2[b], jnp.ones((length, 128), bf16))
        decay = jnp.exp(total[:LK] + total[LK:])
        dhi = decay.astype(bf16)
        dlo = (decay - dhi.astype(f32)).astype(bf16)
        packed = jnp.where(lane < 64, dhi.astype(f32), dlo.astype(f32)).astype(bf16)
        lst[b] = jnp.concatenate([state, packed], axis=1).reshape(NZ, RP, GLA_VALUE + 128)

        @pl.loop(0, NZ)
        def _(r):
            @pl.when(r * NY + b != sp)
            def _():
                piece_copy(b, r, sp).start()

            @pl.when(r * NY + b == sp)
            def _():
                arr[sp] = lst[b, r]

        @pl.when(sp < NS - 1)
        def _():
            halo_copy(b).start()

    with scope("i_y1"):
        y_arrive(1)

    @pl.loop(0, NF)
    def _(i):
        b = order(i)

        @pl.when(i == 1)
        def _():
            with scope("i_xs"):
                for d in range(1, NF):
                    slice_copy(d).wait_recv()
                z_send(2)
                pass_y(2, 0)

        @pl.when(i == 2)
        def _():
            with scope("i_relay1"):
                relay_arrive(1)

        @pl.when(i == 3)
        def _():
            with scope("i_owx"):
                for j in range(2):
                    ow_copy(j).wait_recv()
                    ow_copy(4 + j).start()
                    ow_core(j).start()

        q = query[b].astype(f32) * LK ** -0.5
        k = kkey[b].astype(f32)
        ri = lax.broadcasted_iota(jnp.int32, (length, length), 0)
        ci = lax.broadcasted_iota(jnp.int32, (length, length), 1)
        rk = lax.broadcasted_iota(jnp.int32, (length, LK), 0)
        scores = jnp.where(ri == ci, dot_t(q.astype(bf16), kkey[b]), 0.0)
        for n, h in enumerate(levels):
            decay = jnp.exp(log_sum(n, b))
            later = (rk & h) != 0
            qh = jnp.where(later, q * decay, 0.0).astype(bf16)
            kh = jnp.where(later, 0.0, k * decay).astype(bf16)
            same = (ri & ~(2 * h - 1)) == (ci & ~(2 * h - 1))
            scores = scores + jnp.where(same, dot_t(qh, kh), 0.0)
        reach[b] = (q * jnp.exp(log_sum(len(levels), b))).astype(bf16)
        oacc[b] = dot(scores.astype(bf16), val[b])

    with scope("k_core1"):
        core_all(1).wait_recv()

    def prefix_copy(s):
        return rc(pre.at[s], state_in.at[yy, zz], qs.at[s], qr.at[sp], {"sp": s})

    def scan():
        def step(s, carry):
            @pl.when(s != sp)
            def _():
                piece_copy(0, 0, s).wait_recv()

            pre[s] = carry.astype(bf16)
            x = arr[s].astype(f32)
            g = x[:, GLA_VALUE:]
            g = g + pltpu.roll(g, 64, 1)
            return carry * jnp.concatenate([g, g], axis=1) + x[:, :GLA_VALUE]

        with scope("l_scan"):
            lax.fori_loop(0, NS, step, jnp.zeros((RP, GLA_VALUE), f32))

        @pl.loop(0, NS)
        def _(s):
            @pl.when(s != sp)
            def _():
                prefix_copy(s).start()

            @pl.when(s == sp)
            def _():
                state_in[yy, zz] = pre[s]

    span = length + WINDOW
    row = lax.broadcasted_iota(jnp.int32, (length, span), 0)
    col = lax.broadcasted_iota(jnp.int32, (length, span), 1)
    distance = row - col + WINDOW
    heads = sink.shape[1]
    wq = heads * HEAD_DIM

    def rows_copy(src, dst, ssem, rsem, off):
        return rc(src.at[off], dst.at[lax.rem(NF - off, NF)], ssem.at[off], rsem.at[off], at_f(off))

    def wrow_copy(off):
        return rows_copy(wrow, wall, ws, wr, off)

    def lrow_copy(off):
        return rows_copy(lrow, lall, ls, lr, off)

    @pl.loop(0, NF)
    def _(i):
        b = order(i)
        off = lax.rem(b - f + NF, NF)

        @pl.when(i == 0)
        def _():
            scan()

        @pl.when(i == 1)
        def _():
            with scope("m_z2"):
                z_arrive(2)

        @pl.when(i == 2)
        def _():
            with scope("m_owx2"):
                for j in range(2, 4):
                    ow_copy(j).wait_recv()
                    ow_core(j).start()

        @pl.when(i == 3)
        def _():
            with scope("m_y2"):
                y_arrive(2)

        @pl.when(sp > 0)
        def _():
            halo_copy(b).wait_recv()

        p = dot(toks[b], W2[...].reshape(depth, -1)).astype(bf16)
        allowed = (distance >= 0) & (distance < WINDOW) & ((col >= WINDOW) | (sp > 0))
        kv = kvbuf[b]
        k, v = kv[:, :HEAD_DIM], kv[:, HEAD_DIM:]
        heads_out = []
        for j in range(heads):
            score = dot_t(p[:, j * HEAD_DIM:(j + 1) * HEAD_DIM], k) * HEAD_DIM ** -0.5
            score = jnp.where(allowed, score, -jnp.inf)
            sk = sink[0:1, j:j + 1]
            top = jnp.maximum(jnp.max(score, axis=1, keepdims=True), sk)
            e = jnp.exp(score - top)
            total = jnp.sum(e, axis=1, keepdims=True) + jnp.exp(sk - top)
            heads_out.append((dot(e.astype(bf16), v) / total).astype(bf16))
        gates[b] = p[:, wq:]
        win = jnp.concatenate(heads_out, axis=1)

        @pl.when(i == 0)
        def _():
            wall[0] = win

        @pl.when(i > 0)
        def _():
            wrow[off] = win
            wrow_copy(off).start()

    @pl.loop(0, NF)
    def _(i):
        off = jnp.where(i == 0, 2, jnp.where(i == 1, NF - 1, jnp.where(i == 2, 1, 0)))
        b = lax.rem(f + off, NF)

        with scope("o_state"):
            @pl.loop(0, NZ)
            def _(r):
                o = r * NY + b

                @pl.when(o != sp)
                def _():
                    rc(pre.at[0], state_in.at[b, r], qs.at[0], qr.at[o], {"sp": o}).wait_recv()

        gate = gates[b].astype(f32)
        o = oacc[b] + dot(reach[b], state_in[b].reshape(LK, GLA_VALUE))
        scaled = o * lax.rsqrt(jnp.mean(o * o, axis=1, keepdims=True) + norm_epsilon)
        lin = (scaled * gain[...] * (gate / (1.0 + jnp.exp(-gate)))).astype(bf16)

        @pl.when(off == 0)
        def _():
            lall[0] = lin

        @pl.when(off > 0)
        def _():
            lrow[off] = lin
            lrow_copy(off).start()

    with scope("p_ow"):
        relay_arrive(2)
        for j in range(4, 6):
            ow_copy(j).wait_recv()
            ow_core(j).start()
        ow_core_all().wait_recv()
    with scope("p_wrow"):
        for off in range(1, NF):
            wrow_copy(off).wait_recv()

    chunk = 512

    def project(kind, rows_of, init):
        left = jnp.concatenate([rows_of[n] for n in range(NF)], axis=1)
        for c in range(depth // chunk):
            cs = slice(c * chunk, (c + 1) * chunk)
            y = dot(left, OW[kind * NF:(kind + 1) * NF, :, cs].reshape(NF * orows, chunk))
            if init:
                acc[:, cs] = y
            else:
                out[:, cs] = (acc[:, cs] + y).astype(bf16)

    with scope("q_proj1"):
        project(1, wall, True)
    with scope("r_core2"):
        core_all(2).wait_recv()
    with scope("r_lrow"):
        for off in range(1, NF):
            lrow_copy(off).wait_recv()
    with scope("s_proj2"):
        project(0, lall, False)

    with scope("t_end"):
        for j in range(6):
            token_copy(j).wait_send()
            ow_copy(j).wait_send()
        for d in range(1, NF):
            slice_copy(d).wait_send()
            wrow_copy(d).wait_send()
            lrow_copy(d).wait_send()
        for g in range(3):
            for d in range(1, NZ):
                z_copy(g, d).wait_send()
            for k in range(NZ):
                y_copy(g, k, 0).wait_send()
                y_copy(g, k, 1).wait_send()
                relay_copy(g, k).wait_send()
            core_all(g).wait_send()
        ow_core_all().wait_send()

        @pl.when(sp < NS - 1)
        def _():
            for b in range(NF):
                halo_copy(b).wait_send()

        @pl.loop(0, NS)
        def _(s):
            @pl.when(s != sp)
            def _():
                piece_copy(lax.rem(s, NY), s // NY, sp).wait_send()
                prefix_copy(s).wait_send()


def shards(
    NS, NF, NT,
    tokens, linear_query, linear_key, linear_decay, linear_value, linear_gate, decay_bias,
    norm_gain, window_query, window_key, window_value, sink_logit, linear_output, window_output,
):
    _, length, depth = tokens.shape
    kb = linear_query.shape[0]
    NZ = NS // NY
    levels = []
    h = 1
    while h < length:
        levels.append(h)
        h *= 2
    vm = pltpu.VMEM
    dma = pltpu.SemaphoreType.DMA
    kv_width = window_key.shape[1] + window_value.shape[1]
    width1 = 3 * GLA_KEY + GLA_VALUE + kv_width
    width2 = window_query.shape[1] + GLA_VALUE
    anyspec = pl.BlockSpec(memory_space=pl.ANY)
    vspec = pl.BlockSpec(memory_space=vm)
    result = pl.pallas_call(
        functools.partial(kernel, NS, NF, NT, tuple(levels)),
        out_shape=jax.ShapeDtypeStruct((length, depth), bf16),
        in_specs=[anyspec] * 9 + [vspec] * 5,
        out_specs=vspec,
        scratch_shapes=[
            vm((NF, length, depth), bf16),
            vm((NZ, NY, NT, kb, width1), bf16),
            vm((NZ, NY, NT, kb, width2), bf16),
            vm((2 * NF, linear_output.shape[0], depth), bf16),
            vm((len(levels) + 2, length, length), bf16),
            vm((NF, length, 2 * GLA_KEY), bf16),
            vm((NF, length, GLA_KEY), bf16),
            vm((NF, length, GLA_VALUE), bf16),
            vm((NF, length, GLA_KEY), bf16),
            vm((NF, length + WINDOW, kv_width), bf16),
            vm((NF, NZ, GLA_KEY // NZ, GLA_VALUE + 128), bf16),
            vm((NS, GLA_KEY // NZ, GLA_VALUE + 128), bf16),
            vm((NS, GLA_KEY // NZ, GLA_VALUE), bf16),
            vm((NF, NZ, GLA_KEY // NZ, GLA_VALUE), bf16),
            vm((NF, length, GLA_VALUE), bf16),
            vm((NF, length, window_query.shape[1]), bf16),
            vm((NF, length, GLA_VALUE), bf16),
            vm((NF, length, window_query.shape[1]), bf16),
            vm((NF, length, GLA_VALUE), f32),
            vm((NF, length, GLA_KEY), bf16),
            vm((NF, length, GLA_VALUE), bf16),
            vm((length, depth), f32),
            dma((9,)),
            dma((3, NZ)), dma((3, NZ)),
            dma((3, 2, NZ)), dma((3, 2, NZ)),
            dma((3, NZ)), dma((3, NZ)),
            dma((4,)), dma((4,)),
            dma((6,)), dma((6,)),
            dma((NF,)), dma((NF,)),
            dma((NF, NZ)), dma((NS,)),
            dma((NS,)), dma((NS,)),
            dma((NF,)), dma((NF,)),
            dma((NF,)), dma((NF,)),
            dma((NF,)), dma((NF,)),
            dma((6,)), dma((6,)),
        ],
        compiler_params=pltpu.CompilerParams(
            collective_id=0, has_side_effects=True, vmem_limit_bytes=60 * 1024 * 1024),
        name="layer",
    )(tokens[0], linear_decay, linear_key, linear_value, linear_query, window_query, linear_gate,
      linear_output, window_output, window_key, window_value,
      decay_bias[None], norm_gain[None], sink_logit[None])
    return result[None]


def solution(mesh):
    shape = mesh.shape
    return jax.shard_map(
        functools.partial(shards, shape["sp"], shape["fs"], shape["tp"]),
        mesh=mesh,
        in_specs=(
            P(("fs", "tp"), "sp", None),
            P(("sp", "tp"), "fs"),
            P(("sp", "tp"), "fs"),
            P(("sp", "tp"), "fs"),
            P(("sp", "tp"), "fs"),
            P(("sp", "tp"), "fs"),
            P("fs"),
            P(),
            P(("sp", "tp"), "fs"),
            P(("sp", "tp"), "fs"),
            P(("sp", "tp"), "fs"),
            P("fs"),
            P("fs", None),
            P("fs", None),
        ),
        out_specs=P(("fs", "tp"), "sp", None),
        check_vma=False,
    )
```

time: 107 us -> 83.6 us (0.78); the launches traced: 105 us -> 83.4 us
  Pallas kernels: 103 us -> 81.3 us
    pallas_call x1, Pallas kernels: 103 us -> 81.3 us  [shards(): pl.pallas_call(functools.partial(kernel, NS, NF, NT, tuple(levels)), out_...]
where the time goes in v2:
time: 83.6 us; the launch traced here: 83.4 us
  Pallas kernels  81.3 us (97%)
  local copies, waits for them, and re-layouts  2.09 us (2%)
    pallas_call x1, Pallas kernels, shards(): pl.pallas_call(functools.partial(kernel, NS, NF, NT, tuple(levels)), out_...  81.3 us
    unnamed x1, local copies, waits for them, and re-layouts  2.09 us

profile of v2, /device:TPU:1, one launch (start us, length us, event | category | flops | bytes accessed | tf_op | source)
XLA Modules:
  0.0 83.4 jit_solution(16809645064208379311)
XLA Ops:
  0.0 81.3 %layer.1 = bf16[192,2048]{1,0:T(8,128)(2,1)} custom-call(bf16[192,2048]{1,0:T(8,128)(2,1)} %bitcast.6, bf16[32,128]{1,0:T(8,128)(2,1)} %w_decay.1, bf16[32,128]{1,0:T(8,128)(2,1)} %w_key.1, bf16[32,256]{1,0:T(8,128)(2,1)} %w_value.1, bf16[32,128]{1,0:T(8,128)(2,1)} %w_lq.1, bf16[32,256]{1,0:T(8,128)(2,1)} %w_wq.1, bf16[32,256]{1,0:T(8,128)(2,1)} %w_gate.1, ...), custom_call_target="tpu_custom_call" | custom-call | tf_op jit(solution)/shard_map/layer/pallas_call | solution.py:567
  81.3 2.1 %copy.16 = bf16[1,192,2048]{2,1,0:T(8,128)(2,1)} copy(bf16[1,192,2048]{2,1,0:T(8,128)(2,1)} %bitcast.5) | data formatting | bytes 1572864

commit v3 on v2

--- a/solution.py
+++ b/solution.py
@@ -36,7 +36,7 @@
     out,
     toks, W1, W2, OW, sums, f2, kkey, val, query, kvbuf, lst, arr, pre, state_in,
     lrow, wrow, lall, wall, oacc, reach, gates, acc,
-    lsem, zs, zr, ys, yr, rs, rr, dsnd, drcv, ts, tr, hs, hr, asnd, arcv, qs, qr,
+    obuf, lsem, zs, zr, ys, yr, rs, rr, dsnd, drcv, ts, tr, hs, hr, asnd, arcv, qs, qr,
     ls, lr, ws, wr, xs, xr, os, orr,
 ):
     sp, f, t = lax.axis_index("sp"), lax.axis_index("fs"), lax.axis_index("tp")
@@ -145,7 +145,7 @@
 
     def slice_copy(d):
         r, c = ow_tile(0, 0)
-        return rc(OW.at[0, r, c], OW.at[NF - d, r, c], xs.at[d], xr.at[d], at_f(d))
+        return rc(lin_o.at[r, c], OW.at[NF - d, r, c], xs.at[d], xr.at[d], at_f(d))
 
     def slot(g, k, yo):
         if g == 2:
@@ -187,8 +187,8 @@
         y_copy(g, k, 1).start()
         core_copy(g, k, 0).start()
 
-    def z_arrive(g):
-        for k in zorder:
+    def z_arrive(g, ks=None):
+        for k in zorder if ks is None else ks:
             z_copy(g, k).wait_recv()
             pass_y(g, k)
 
@@ -208,6 +208,8 @@
             relay_copy(g, k).wait_recv()
             core_copy(g, k, 2).start()
 
+    for d in range(1, NF):
+        slice_copy(d).start()
     z_send(0)
     for j in range(2):
         token_copy(j).start()
@@ -221,10 +223,12 @@
         for j in range(2):
             token_copy(j).wait_recv()
             token_copy(4 + j).start()
+    with scope("d_slices"):
+        for d in range(1, NF):
+            slice_copy(d).wait_recv()
+    z_send(2)
     for c in local[7:]:
         c.wait()
-    for d in range(1, NF):
-        slice_copy(d).start()
     for j in range(4):
         ow_copy(j).start()
     with scope("e_y0"):
@@ -234,6 +238,7 @@
         z_arrive(1)
     with scope("f_relay0"):
         relay_arrive(0)
+    pass_y(2, 0)
     with scope("g_core0"):
         core_all(0).wait_recv()
 
@@ -266,6 +271,8 @@
         def _():
             with scope("h_tok2"):
                 token_copy(3).wait_recv()
+            with scope("i_y1"):
+                y_arrive(1)
 
         @pl.when(i == 3)
         def _():
@@ -307,8 +314,8 @@
         def _():
             halo_copy(b).start()
 
-    with scope("i_y1"):
-        y_arrive(1)
+    with scope("i_z2"):
+        z_arrive(2)
 
     @pl.loop(0, NF)
     def _(i):
@@ -316,24 +323,8 @@
 
         @pl.when(i == 1)
         def _():
-            with scope("i_xs"):
-                for d in range(1, NF):
-                    slice_copy(d).wait_recv()
-                z_send(2)
-                pass_y(2, 0)
-
-        @pl.when(i == 2)
-        def _():
             with scope("i_relay1"):
                 relay_arrive(1)
-
-        @pl.when(i == 3)
-        def _():
-            with scope("i_owx"):
-                for j in range(2):
-                    ow_copy(j).wait_recv()
-                    ow_copy(4 + j).start()
-                    ow_core(j).start()
 
         q = query[b].astype(f32) * LK ** -0.5
         k = kkey[b].astype(f32)
@@ -382,12 +373,13 @@
             def _():
                 state_in[yy, zz] = pre[s]
 
-    span = length + WINDOW
-    row = lax.broadcasted_iota(jnp.int32, (length, span), 0)
-    col = lax.broadcasted_iota(jnp.int32, (length, span), 1)
-    distance = row - col + WINDOW
-    heads = sink.shape[1]
-    wq = heads * HEAD_DIM
+    QB = 64
+    row = lax.rem(lax.broadcasted_iota(jnp.int32, (2 * QB, QB + WINDOW), 0), QB)
+    col = lax.broadcasted_iota(jnp.int32, (2 * QB, QB + WINDOW), 1)
+    band = (col > row) & (col <= row + WINDOW)
+    lane_q = lax.broadcasted_iota(jnp.int32, (2 * QB, 128), 1)
+    lane_k = lax.broadcasted_iota(jnp.int32, (QB + WINDOW, 128), 1)
+    wq = sink.shape[1] * HEAD_DIM
 
     def rows_copy(src, dst, ssem, rsem, off):
         return rc(src.at[off], dst.at[lax.rem(NF - off, NF)], ssem.at[off], rsem.at[off], at_f(off))
@@ -403,21 +395,17 @@
         b = order(i)
         off = lax.rem(b - f + NF, NF)
 
-        @pl.when(i == 0)
+        @pl.when(i == 1)
+        def _():
+            with scope("i_owx"):
+                for j in range(2):
+                    ow_copy(j).wait_recv()
+                    ow_copy(4 + j).start()
+                    ow_core(j).start()
+
+        @pl.when(i == 2)
         def _():
             scan()
-
-        @pl.when(i == 1)
-        def _():
-            with scope("m_z2"):
-                z_arrive(2)
-
-        @pl.when(i == 2)
-        def _():
-            with scope("m_owx2"):
-                for j in range(2, 4):
-                    ow_copy(j).wait_recv()
-                    ow_core(j).start()
 
         @pl.when(i == 3)
         def _():
@@ -428,21 +416,38 @@
         def _():
             halo_copy(b).wait_recv()
 
-        p = dot(toks[b], W2[...].reshape(depth, -1)).astype(bf16)
-        allowed = (distance >= 0) & (distance < WINDOW) & ((col >= WINDOW) | (sp > 0))
-        kv = kvbuf[b]
-        k, v = kv[:, :HEAD_DIM], kv[:, HEAD_DIM:]
-        heads_out = []
-        for j in range(heads):
-            score = dot_t(p[:, j * HEAD_DIM:(j + 1) * HEAD_DIM], k) * HEAD_DIM ** -0.5
-            score = jnp.where(allowed, score, -jnp.inf)
-            sk = sink[0:1, j:j + 1]
-            top = jnp.maximum(jnp.max(score, axis=1, keepdims=True), sk)
-            e = jnp.exp(score - top)
-            total = jnp.sum(e, axis=1, keepdims=True) + jnp.exp(sk - top)
-            heads_out.append((dot(e.astype(bf16), v) / total).astype(bf16))
-        gates[b] = p[:, wq:]
-        win = jnp.concatenate(heads_out, axis=1)
+        p = dot(toks[b], W2[...].reshape(depth, -1))
+        gates[b] = p[:, wq:].astype(bf16)
+        q = (p[:, :wq].astype(bf16).astype(f32) * HEAD_DIM ** -0.5).astype(bf16)
+        zero = jnp.zeros((), bf16)
+        one = jnp.ones((), bf16)
+        blocks = []
+        for n in range(length // QB):
+            qn = q[n * QB:(n + 1) * QB]
+            stacked = jnp.concatenate([qn[:, :128], qn[:, 128:]], axis=0)
+            kv = kvbuf[b, n * QB:n * QB + QB + WINDOW, :]
+            swapped = jnp.concatenate([kv[:, HEAD_DIM:], kv[:, :HEAD_DIM]], axis=1)
+            allowed = band
+            if n * QB < WINDOW:
+                allowed = band & ((col >= WINDOW - n * QB) | (sp > 0))
+            parts, fades = [], []
+            for odd in range(2):
+                mine = (lane_q >= HEAD_DIM) if odd else (lane_q < HEAD_DIM)
+                score = dot_t(jnp.where(mine, stacked, zero), swapped if odd else kv)
+                score = jnp.where(allowed, score, -jnp.inf)
+                sk = jnp.concatenate([jnp.broadcast_to(sink[0:1, odd:odd + 1], (QB, 1)),
+                                      jnp.broadcast_to(sink[0:1, 2 + odd:3 + odd], (QB, 1))], axis=0)
+                top = jnp.maximum(jnp.max(score, axis=1, keepdims=True), sk)
+                e = jnp.exp(score - top).astype(bf16)
+                fades.append(jnp.exp(sk - top))
+                ext = jnp.where((lane_k >= HEAD_DIM) if odd else (lane_k < HEAD_DIM), kv if odd else swapped, one)
+                parts.append(dot(e, ext))
+            low = lane_q < HEAD_DIM
+            num = jnp.where(low, parts[0], parts[1])
+            den = pltpu.roll(jnp.where(low, parts[1], parts[0]), HEAD_DIM, 1) + jnp.where(low, fades[0], fades[1])
+            res = (num / den).astype(bf16)
+            blocks.append(jnp.concatenate([res[:QB], res[QB:]], axis=1))
+        win = jnp.concatenate(blocks, axis=0)
 
         @pl.when(i == 0)
         def _():
@@ -483,7 +488,7 @@
 
     with scope("p_ow"):
         relay_arrive(2)
-        for j in range(4, 6):
+        for j in range(2, 6):
             ow_copy(j).wait_recv()
             ow_core(j).start()
         ow_core_all().wait_recv()
@@ -492,6 +497,10 @@
             wrow_copy(off).wait_recv()
 
     chunk = 512
+
+    def out_copy(c):
+        cs = pl.ds(c * chunk, chunk)
+        return pltpu.make_async_copy(obuf.at[:, cs], out.at[:, cs], lsem.at[9 + c])
 
     def project(kind, rows_of, init):
         left = jnp.concatenate([rows_of[n] for n in range(NF)], axis=1)
@@ -501,7 +510,8 @@
             if init:
                 acc[:, cs] = y
             else:
-                out[:, cs] = (acc[:, cs] + y).astype(bf16)
+                obuf[:, cs] = (acc[:, cs] + y).astype(bf16)
+                out_copy(c).start()
 
     with scope("q_proj1"):
         project(1, wall, True)
@@ -514,6 +524,8 @@
         project(0, lall, False)
 
     with scope("t_end"):
+        for c in range(depth // chunk):
+            out_copy(c).wait()
         for j in range(6):
             token_copy(j).wait_send()
             ow_copy(j).wait_send()
@@ -568,7 +580,7 @@
         functools.partial(kernel, NS, NF, NT, tuple(levels)),
         out_shape=jax.ShapeDtypeStruct((length, depth), bf16),
         in_specs=[anyspec] * 9 + [vspec] * 5,
-        out_specs=vspec,
+        out_specs=anyspec,
         scratch_shapes=[
             vm((NF, length, depth), bf16),
             vm((NZ, NY, NT, kb, width1), bf16),
@@ -592,7 +604,8 @@
             vm((NF, length, GLA_KEY), bf16),
             vm((NF, length, GLA_VALUE), bf16),
             vm((length, depth), f32),
-            dma((9,)),
+            vm((length, depth), bf16),
+            dma((9 + 4,)),
             dma((3, NZ)), dma((3, NZ)),
             dma((3, 2, NZ)), dma((3, 2, NZ)),
             dma((3, NZ)), dma((3, NZ)),

time: 83.6 us -> 76.4 us (0.914)
  Pallas kernels: 81.3 us -> 74 us
    pallas_call x1, Pallas kernels: 81.3 us -> 74 us  [shards(): pl.pallas_call(functools.partial(kernel, NS, NF, NT, tuple(levels)), out_...]
where the time goes in v3:
time: 76.4 us; the launch traced here: 76.1 us
  Pallas kernels  74 us (97%)
  local copies, waits for them, and re-layouts  2.09 us (3%)
    pallas_call x1, Pallas kernels, shards(): pl.pallas_call(functools.partial(kernel, NS, NF, NT, tuple(levels)), out_...  74 us
    unnamed x1, local copies, waits for them, and re-layouts  2.09 us

profile of v3, /device:TPU:1, one launch (start us, length us, event | category | flops | bytes accessed | tf_op | source)
XLA Modules:
  0.0 76.1 jit_solution(13852607936889827174)
XLA Ops:
  0.0 74.0 %layer.1 = bf16[192,2048]{1,0:T(8,128)(2,1)} custom-call(bf16[192,2048]{1,0:T(8,128)(2,1)} %bitcast.6, bf16[32,128]{1,0:T(8,128)(2,1)} %w_decay.1, bf16[32,128]{1,0:T(8,128)(2,1)} %w_key.1, bf16[32,256]{1,0:T(8,128)(2,1)} %w_value.1, bf16[32,128]{1,0:T(8,128)(2,1)} %w_lq.1, bf16[32,256]{1,0:T(8,128)(2,1)} %w_wq.1, bf16[32,256]{1,0:T(8,128)(2,1)} %w_gate.1, ...), custom_call_target="tpu_custom_call" | custom-call | tf_op jit(solution)/shard_map/layer/pallas_call | solution.py:579
  74.0 2.1 %copy.16 = bf16[1,192,2048]{2,1,0:T(8,128)(2,1)} copy(bf16[1,192,2048]{2,1,0:T(8,128)(2,1)} %bitcast.5) | data formatting | bytes 1572864

commit v4 on v3

v4 whole, which is shorter than its diff:
```python
import functools

import jax
import jax.numpy as jnp
from jax import lax
from jax.experimental import pallas as pl
from jax.experimental.pallas import tpu as pltpu
from jax.sharding import PartitionSpec as P

GLA_KEY = 128
GLA_VALUE = 256
HEAD_DIM = 64
WINDOW = 128
NY = 4
XR = 128

norm_epsilon = 1e-05
MESH = pl.DeviceIdType.MESH
f32, bf16 = jnp.float32, jnp.bfloat16


def dot(a, b):
    return jnp.dot(a, b, preferred_element_type=f32)


def dot_t(a, b):
    return lax.dot_general(a, b, (((1,), (1,)), ((), ())), preferred_element_type=f32)


def dot_rows(a, b):
    return lax.dot_general(a, b, (((0,), (0,)), ((), ())), preferred_element_type=f32)


def kernel(
    NS, NF, NT, levels,
    tok, w_decay, w_key, w_value, w_lq, w_wq, w_gate, lin_o, win_o, w_wk, w_wv, bias, gain, sink,
    out,
    toks, W1, W2, OW, sums, f2, kkey, val, query, kvbuf, lst, arr, pre, state_in,
    lrow, wrow, lall, wall, oacc, reach, gates, acc, obuf, sc, eb,
    lsem, zs, zr, ys, yr, rr, dsnd, drcv, ts, tr, hs, hr, asnd, arcv, qs, qr,
    ls, lr, ws, wr, xs, xr, os, orr,
):
    sp, f, t = lax.axis_index("sp"), lax.axis_index("fs"), lax.axis_index("tp")
    NZ = NS // NY
    HZ = NZ // 2
    zz, yy = sp // NY, lax.rem(sp, NY)
    length, depth = tok.shape
    half = length // 2
    tau = NS * length // 16
    LK = GLA_KEY
    RP = LK // NZ
    groups = (W1, W2)
    scope = jax.named_scope

    def at_z(d):
        return {"sp": lax.rem(zz + d, NZ) * NY + yy}

    def at_y(d):
        return {"sp": zz * NY + lax.rem(yy + d, NY)}

    def at_f(d):
        return {"fs": lax.rem(f + d, NF)}

    other = {"tp": 1 - t}

    def rc(src, dst, ssem, rsem, dev):
        return pltpu.make_async_remote_copy(
            src_ref=src, dst_ref=dst, send_sem=ssem, recv_sem=rsem, device_id=dev, device_id_type=MESH)

    def got(ref, sem):
        rc(ref, ref, sem, sem, other).wait_recv()

    def gone(ref, sem):
        rc(ref, ref, sem, sem, other).wait_send()

    barrier = pltpu.get_barrier_semaphore()
    greet = [at_z(d) for d in range(1, NZ)] + [at_y(1), at_y(NY - 1)] + [at_f(d) for d in range(1, NF)] + [other]
    for dev in greet:
        pl.semaphore_signal(barrier, inc=1, device_id=dev, device_id_type=MESH)
    own1, own2 = W1.at[zz, yy, t], W2.at[zz, yy, t]
    lin_rows = lin_o.shape[0]
    orows = OW.shape[1]
    loads = [
        (tok, toks.at[f]),
        (w_decay, own1.at[:, 0:128]), (w_key, own1.at[:, 128:256]), (w_value, own1.at[:, 256:512]),
        (w_lq, own1.at[:, 512:640]),
        (w_wq, own2.at[:, 0:256]), (w_gate, own2.at[:, 256:512]),
        (lin_o, OW.at[0, 0:lin_rows]), (win_o, OW.at[0, lin_rows:orows]),
    ]
    local = [pltpu.make_async_copy(a, b, lsem.at[n]) for n, (a, b) in enumerate(loads)]
    for c in local:
        c.start()
    W1[zz, yy, t, :, 640:768] = jnp.concatenate([w_wk[...], w_wv[...]], axis=1)

    i0 = lax.broadcasted_iota(jnp.int32, (length, length), 0)
    s0 = lax.broadcasted_iota(jnp.int32, (length, length), 1)
    for n, h in enumerate(levels):
        ref = (i0 & ~(2 * h - 1)) + h - 1
        later = (i0 & h) != 0
        low = jnp.where(later, ref, i0)
        high = jnp.where(later, i0, ref)
        sums[n] = jnp.where((s0 > low) & (s0 <= high), 1.0, 0.0).astype(bf16)
    sums[len(levels)] = jnp.where(s0 <= i0, 1.0, 0.0).astype(bf16)
    sums[len(levels) + 1] = jnp.where(s0 > i0, 1.0, 0.0).astype(bf16)

    @pl.when(sp == 0)
    def _():
        kvbuf[:, 0:WINDOW, :] = jnp.zeros((NF, WINDOW, kvbuf.shape[2]), bf16)

    with scope("a_loads"):
        for c in local:
            c.wait()
    with scope("b_barrier"):
        pl.semaphore_wait(barrier, len(greet))

    def x_step(j):
        return j in (0, 2, 4), j in (0, 3, 4)

    def token_part(who, first):
        return toks.at[who, pl.ds(0 if first else half, half)]

    def token_send(j):
        right, first = x_step(j)
        who = f if j < 4 else lax.rem(f + (NF - 1 if right else 1), NF)
        ref = token_part(who, first)
        rc(ref, ref, ts.at[0], tr.at[min(j, 4)], at_f(1 if right else NF - 1)).start()

    ocols = depth // NT
    ZR = orows - XR
    cols_t = pl.ds(pl.multiple_of(t * ocols, ocols), ocols)

    def ow_part(rel, first):
        return OW.at[rel, pl.ds(ZR + (0 if first else XR // 2), XR // 2), cols_t]

    def ow_send(j):
        right, first = x_step(j)
        src = 0 if j < 4 else (NF - 1 if right else 1)
        dst = (src + (NF - 1 if right else 1)) % NF
        rc(ow_part(src, first), ow_part(dst, first), os.at[0], orr.at[min(j, 2)],
           at_f(1 if right else NF - 1)).start()

    ow_x = OW.at[pl.ds(1, NF - 1), pl.ds(ZR, XR), cols_t]
    tile_r = ZR // NZ
    tile_c = ocols // NY

    def ow_cols(yo):
        y1 = lax.rem(yy + NY - yo, NY)
        return pl.ds(pl.multiple_of(t * ocols + y1 * tile_c, tile_c), tile_c)

    def ow_rows(z, count):
        return pl.ds(pl.multiple_of(z * tile_r, tile_r), count * tile_r)

    def shard(g, k, yo):
        z1 = lax.rem(zz - k + NZ, NZ)
        if g == 2:
            return OW.at[pl.ds(1, NF - 1), ow_rows(z1, 1), ow_cols(yo)]
        return groups[g].at[z1, lax.rem(yy - yo + NY, NY), t]

    def box(g, z, count, yo):
        if g == 2:
            return OW.at[pl.ds(1, NF - 1), pl.ds(z * tile_r, count * tile_r), ow_cols(yo)]
        return groups[g].at[pl.ds(z, count), lax.rem(yy - yo + NY, NY), t]

    def whole(g, ycount):
        if g == 2:
            return OW.at[pl.ds(1, NF - 1), pl.ds(0, ZR), pl.ds(0, ycount * tile_c)]
        return groups[g].at[:, pl.ds(0, ycount), t]

    pairs = [[0]] + [[d, NZ - d] for d in range(1, HZ)] + [[HZ]]
    ZW = len(pairs)
    zorder = [d for p in pairs[1:] for d in p]
    left, right = 1, NY - 1

    def y_sem(g, side, part):
        return yr.at[side, part if g == 0 else (ZW if g == 1 else ZW + 1 + part)]

    def z_send(g):
        ref = shard(g, 0, 0)
        for p in range(1, ZW):
            for d in pairs[p]:
                rc(ref, ref, zs.at[g], zr.at[p - 1 if g == 0 else ZW - 2 + g], at_z(d)).start()

    def pass_y(g, ref, part):
        rc(ref, ref, ys.at[g], y_sem(g, 0, part), at_y(1)).start()
        rc(ref, ref, ys.at[g], y_sem(g, 1, part), at_y(NY - 1)).start()

    def relay(g, ref, up):
        rc(ref, ref, ys.at[g], rr.at[g], at_y(1 if up else NY - 1)).start()

    def core_send(g, ref):
        rc(ref, ref, dsnd.at[g], drcv.at[g], other).start()

    def core_box(g, yo):
        core_send(g, box(g, 0, NZ, yo))

    def z_arrive(g):
        got(box(g, 0, NZ - 1, 0), zr.at[ZW - 2 + g])
        core_box(g, 0)

    def relay_arrive(g):
        got(box(g, 0, NZ, 2), rr.at[g])
        core_box(g, 2)

    def slice_send(d):
        r, c = ow_rows(zz, 1), ow_cols(0)
        rc(OW.at[0, r, c], OW.at[NF - d, r, c], xs.at[0], xr.at[0], at_f(d)).start()

    slices = OW.at[pl.ds(1, NF - 1), ow_rows(zz, 1), ow_cols(0)]

    for d in range(1, NF):
        slice_send(d)
    z_send(0)
    for j in range(2):
        token_send(j)
    pass_y(0, shard(0, 0, 0), 0)
    for j in range(2, 4):
        token_send(j)
    z_send(1)
    with scope("c_z0"):
        for p in range(1, ZW):
            got(box(0, 0, len(pairs[p]), 0), zr.at[p - 1])
            for k in pairs[p]:
                pass_y(0, shard(0, k, 0), p)
        core_box(0, 0)
    with scope("d_tokfwd"):
        for j in range(2):
            got(token_part(f, True), tr.at[j])
            token_send(4 + j)
    with scope("d_slices"):
        got(slices, xr.at[0])
    z_send(2)
    for j in range(4):
        ow_send(j)
    with scope("e_y0"):
        for p in range(ZW):
            side = p % 2
            got(box(0, 0, len(pairs[p]), 0), y_sem(0, side, p))
            for k in pairs[p]:
                relay(0, shard(0, k, right if side else left), side == 0)
        for p in range(ZW):
            got(box(0, 0, len(pairs[p]), 0), y_sem(0, 1 - p % 2, p))
        core_box(0, left)
        core_box(0, right)
    with scope("e_z1"):
        z_arrive(1)
        pass_y(1, box(1, 0, NZ, 0), 0)
    with scope("f_relay0"):
        relay_arrive(0)
    with scope("g_core0"):
        got(whole(0, NY), drcv.at[0])

    def y_arrive1():
        got(box(1, 0, NZ, 0), y_sem(1, 0, 0))
        relay(1, box(1, 0, HZ, left), True)
        core_box(1, left)
        got(box(1, 0, NZ, 0), y_sem(1, 1, 0))
        relay(1, box(1, HZ, HZ, right), False)
        core_box(1, right)

    def y_arrive2(part):
        if part == 0:
            got(box(2, 0, HZ, 0), y_sem(2, 0, 0))
            relay(2, box(2, 0, HZ, left), True)
            got(box(2, 0, HZ, 0), y_sem(2, 1, 0))
        else:
            got(box(2, 0, HZ, 0), y_sem(2, 1, 1))
            relay(2, box(2, HZ, HZ, right), False)
            got(box(2, 0, HZ, 0), y_sem(2, 0, 1))
            core_box(2, left)
            core_box(2, right)

    def order(i):
        return lax.rem(f + jnp.where(i == 0, 0, jnp.where(i == 1, NF - 1, i - 1)), NF)

    def log_sum(n, b):
        x = dot(sums[n], f2[b])
        return x[:, :LK] + x[:, LK:]

    lane = lax.broadcasted_iota(jnp.int32, (LK, 128), 1)

    @pl.loop(0, NF)
    def _(i):
        b = order(i)

        @pl.when(i == 1)
        def _():
            with scope("h_tok1"):
                got(token_part(f, True), tr.at[2])

        @pl.when(i == 2)
        def _():
            with scope("h_tok2"):
                got(token_part(f, True), tr.at[3])
            with scope("i_y1"):
                y_arrive1()
            with scope("i_z2"):
                z_arrive(2)
                pass_y(2, box(2, 0, HZ, 0), 0)

        @pl.when(i == 3)
        def _():
            with scope("h_tok3"):
                got(toks.at[f], tr.at[4])

        p = dot(toks[b], W1[...].reshape(depth, -1)).astype(bf16)
        x = p[:, :LK].astype(f32) + bias[...]
        forget = (jnp.minimum(x, 0.0) - jnp.log1p(jnp.exp(-jnp.abs(x)))) / tau
        hi = forget.astype(bf16)
        f2[b] = jnp.concatenate([hi, (forget - hi.astype(f32)).astype(bf16)], axis=1)
        k = p[:, LK:2 * LK]
        v = p[:, 2 * LK:2 * LK + GLA_VALUE]
        kkey[b] = k
        val[b] = v
        query[b] = p[:, 512:640]
        kvbuf[b, WINDOW:, :] = p[:, 640:]
        faded = (k.astype(f32) * jnp.exp(log_sum(len(levels) + 1, b))).astype(bf16)
        state = dot_rows(faded, v).astype(bf16)
        total = dot_rows(f2[b], jnp.ones((length, 128), bf16))
        decay = jnp.exp(total[:LK] + total[LK:])
        dhi = decay.astype(bf16)
        dlo = (decay - dhi.astype(f32)).astype(bf16)
        packed = jnp.where(lane < 64, dhi.astype(f32), dlo.astype(f32)).astype(bf16)
        lst[b] = jnp.concatenate([state, packed], axis=1).reshape(NZ, RP, GLA_VALUE + 128)

        @pl.loop(0, NZ)
        def _(r):
            @pl.when(r * NY + b != sp)
            def _():
                rc(lst.at[b, r], arr.at[sp], asnd.at[0], arcv.at[0], {"sp": r * NY + b}).start()

            @pl.when(r * NY + b == sp)
            def _():
                arr[sp] = lst[b, r]

        @pl.when(sp < NS - 1)
        def _():
            rc(kvbuf.at[b, pl.ds(length, WINDOW)], kvbuf.at[b, pl.ds(0, WINDOW)], hs.at[0], hr.at[0],
               {"sp": lax.rem(sp + 1, NS)}).start()

    pass_y(2, box(2, HZ, HZ, 0), 1)

    @pl.loop(0, NF)
    def _(i):
        b = order(i)

        @pl.when(i == 1)
        def _():
            with scope("i_relay1"):
                relay_arrive(1)

        @pl.when(i == 3)
        def _():
            with scope("i_y2"):
                y_arrive2(0)

        q = query[b].astype(f32) * LK ** -0.5
        k = kkey[b].astype(f32)
        ri = lax.broadcasted_iota(jnp.int32, (length, length), 0)
        ci = lax.broadcasted_iota(jnp.int32, (length, length), 1)
        rk = lax.broadcasted_iota(jnp.int32, (length, LK), 0)
        scores = jnp.where(ri == ci, dot_t(q.astype(bf16), kkey[b]), 0.0)
        for n, h in enumerate(levels):
            decay = jnp.exp(log_sum(n, b))
            later = (rk & h) != 0
            qh = jnp.where(later, q * decay, 0.0).astype(bf16)
            kh = jnp.where(later, 0.0, k * decay).astype(bf16)
            same = (ri & ~(2 * h - 1)) == (ci & ~(2 * h - 1))
            scores = scores + jnp.where(same, dot_t(qh, kh), 0.0)
        reach[b] = (q * jnp.exp(log_sum(len(levels), b))).astype(bf16)
        oacc[b] = dot(scores.astype(bf16), val[b])

    with scope("k_core1"):
        got(whole(1, NY), drcv.at[1])
    with scope("i_owx"):
        for j in range(2):
            got(ow_part(0, True), orr.at[j])
            ow_send(4 + j)

    def scan():
        with scope("l_scan"):
            got(arr.at[pl.ds(0, NS - 1)], arcv.at[0])

        unroll = 8

        def step(n, carry):
            for m in range(unroll):
                s = n * unroll + m
                pre[s] = carry.astype(bf16)
                x = arr[s].astype(f32)
                g = x[:, GLA_VALUE:]
                g = g + pltpu.roll(g, 64, 1)
                carry = carry * jnp.concatenate([g, g], axis=1) + x[:, :GLA_VALUE]
            return carry

        with scope("l_scan2"):
            lax.fori_loop(0, NS // unroll, step, jnp.zeros((RP, GLA_VALUE), f32))
            state_in[yy, zz] = pre[sp]

            @pl.loop(1, NS)
            def _(n):
                s = lax.rem(sp + n, NS)
                rc(pre.at[s], state_in.at[yy, zz], qs.at[0], qr.at[yy], {"sp": s}).start()

    QB = 64
    units = 2 * (length // QB)
    row = lax.rem(lax.broadcasted_iota(jnp.int32, (2 * QB, QB + WINDOW), 0), QB)
    col = lax.broadcasted_iota(jnp.int32, (2 * QB, QB + WINDOW), 1)
    band = (col > row) & (col <= row + WINDOW)
    lane_q = lax.broadcasted_iota(jnp.int32, (2 * QB, 128), 1)
    lane_k = lax.broadcasted_iota(jnp.int32, (QB + WINDOW, 128), 1)
    row_k = lax.broadcasted_iota(jnp.int32, (QB + WINDOW, 128), 0)
    wq = sink.shape[1] * HEAD_DIM

    def rows_send(src, dst, ssem, rsem, off):
        rc(src.at[off], dst.at[lax.rem(NF - off, NF)], ssem.at[0], rsem.at[0], at_f(off)).start()

    @pl.when(sp > 0)
    def _():
        with scope("k_halo"):
            got(kvbuf.at[:, pl.ds(0, WINDOW)], hr.at[0])

    @pl.loop(0, NF)
    def _(i):
        b = order(i)
        off = lax.rem(b - f + NF, NF)

        @pl.when(i == 2)
        def _():
            scan()

        @pl.when(i == 3)
        def _():
            with scope("m_y2"):
                y_arrive2(1)

        p = dot(toks[b], W2[...].reshape(depth, -1))
        gates[b] = p[:, wq:].astype(bf16)
        q = (p[:, :wq].astype(bf16).astype(f32) * HEAD_DIM ** -0.5).astype(bf16)
        zero = jnp.zeros((), bf16)
        one = jnp.ones((), bf16)

        def keys(n):
            kv = kvbuf[b, n * QB:n * QB + QB + WINDOW, :]
            return kv, jnp.concatenate([kv[:, HEAD_DIM:], kv[:, :HEAD_DIM]], axis=1)

        for n in range(length // QB):
            qn = q[n * QB:(n + 1) * QB]
            stacked = jnp.concatenate([qn[:, :128], qn[:, 128:]], axis=0)
            kv, swapped = keys(n)
            allowed = band
            if n * QB < WINDOW:
                allowed = band & ((col >= WINDOW - n * QB) | (sp > 0))
            for odd in range(2):
                mine = (lane_q >= HEAD_DIM) if odd else (lane_q < HEAD_DIM)
                score = dot_t(jnp.where(mine, stacked, zero), swapped if odd else kv)
                sk = jnp.concatenate([jnp.broadcast_to(sink[0:1, odd:odd + 1], (QB, 1)),
                                      jnp.broadcast_to(sink[0:1, 2 + odd:3 + odd], (QB, 1))], axis=0)
                sc[2 * n + odd] = jnp.where(allowed, score, jnp.where(col == 0, sk, -jnp.inf))
        for u in range(units):
            score = sc[u]
            eb[u] = jnp.exp(score - jnp.max(score, axis=1, keepdims=True)).astype(bf16)
        blocks = []
        for n in range(length // QB):
            kv, swapped = keys(n)
            parts = []
            for odd in range(2):
                vals = jnp.where(row_k == 0, zero, kv if odd else swapped)
                ext = jnp.where((lane_k >= HEAD_DIM) if odd else (lane_k < HEAD_DIM), vals, one)
                parts.append(dot(eb[2 * n + odd], ext))
            low = lane_q < HEAD_DIM
            num = jnp.where(low, parts[0], parts[1])
            den = pltpu.roll(jnp.where(low, parts[1], parts[0]), HEAD_DIM, 1)
            res = (num / den).astype(bf16)
            blocks.append(jnp.concatenate([res[:QB], res[QB:]], axis=1))
        win = jnp.concatenate(blocks, axis=0)

        @pl.when(i == 0)
        def _():
            wall[0] = win

        @pl.when(i > 0)
        def _():
            wrow[off] = win
            rows_send(wrow, wall, ws, wr, off)

    with scope("n_ow"):
        relay_arrive(2)
        got(OW.at[pl.ds(1, 2), pl.ds(ZR, XR), cols_t], orr.at[2])
        core_send(3, ow_x)

    @pl.loop(0, NF)
    def _(i):
        off = jnp.where(i == 0, 2, jnp.where(i == 1, NF - 1, jnp.where(i == 2, 1, 0)))
        b = lax.rem(f + off, NF)

        with scope("o_state"):
            @pl.when(b != yy)
            def _():
                got(state_in.at[b], qr.at[b])

            @pl.when(b == yy)
            def _():
                got(state_in.at[b, pl.ds(0, NZ - 1)], qr.at[b])

        gate = gates[b].astype(f32)
        o = oacc[b] + dot(reach[b], state_in[b].reshape(LK, GLA_VALUE))
        scaled = o * lax.rsqrt(jnp.mean(o * o, axis=1, keepdims=True) + norm_epsilon)
        lin = (scaled * gain[...] * (gate / (1.0 + jnp.exp(-gate)))).astype(bf16)

        @pl.when(off == 0)
        def _():
            lall[0] = lin

        @pl.when(off > 0)
        def _():
            lrow[off] = lin
            rows_send(lrow, lall, ls, lr, off)

    with scope("p_ow"):
        got(whole(2, NY), drcv.at[2])
        got(ow_x, drcv.at[3])
    with scope("p_wrow"):
        got(wall.at[pl.ds(1, NF - 1)], wr.at[0])

    chunk = 512

    def out_copy(c):
        cs = pl.ds(c * chunk, chunk)
        return pltpu.make_async_copy(obuf.at[:, cs], out.at[:, cs], lsem.at[c])

    def project(lo, hi, rows_of, init):
        lhs = jnp.concatenate([rows_of[n] for n in range(NF)], axis=1)
        for c in range(depth // chunk):
            cs = slice(c * chunk, (c + 1) * chunk)
            y = dot(lhs, OW[:, lo:hi, cs].reshape(-1, chunk))
            if init:
                acc[:, cs] = y
            else:
                obuf[:, cs] = (acc[:, cs] + y).astype(bf16)
                out_copy(c).start()

    with scope("q_proj1"):
        project(lin_rows, orows, wall, True)
    with scope("r_lrow"):
        got(lall.at[pl.ds(1, NF - 1)], lr.at[0])
    with scope("s_proj2"):
        project(0, lin_rows, lall, False)

    with scope("t_end"):
        gone(toks.at[pl.ds(0, NF - 1)], ts.at[0])
        gone(ow_x, os.at[0])
        gone(slices, xs.at[0])
        gone(wrow.at[pl.ds(1, NF - 1)], ws.at[0])
        gone(lrow.at[pl.ds(1, NF - 1)], ls.at[0])
        for g in range(3):
            gone(box(g, 0, NZ - 1, 0), zs.at[g])
            gone(whole(g, 3), ys.at[g])
            gone(whole(g, NY), dsnd.at[g])
        gone(ow_x, dsnd.at[3])
        gone(arr.at[pl.ds(0, NS - 1)], asnd.at[0])
        gone(pre.at[pl.ds(0, NS - 1)], qs.at[0])

        @pl.when(sp < NS - 1)
        def _():
            gone(kvbuf.at[:, pl.ds(0, WINDOW)], hs.at[0])

        for c in range(depth // chunk):
            out_copy(c).wait()


def shards(
    NS, NF, NT,
    tokens, linear_query, linear_key, linear_decay, linear_value, linear_gate, decay_bias,
    norm_gain, window_query, window_key, window_value, sink_logit, linear_output, window_output,
):
    _, length, depth = tokens.shape
    kb = linear_query.shape[0]
    NZ = NS // NY
    levels = []
    h = 1
    while h < length:
        levels.append(h)
        h *= 2
    vm = pltpu.VMEM
    dma = pltpu.SemaphoreType.DMA
    kv_width = window_key.shape[1] + window_value.shape[1]
    width1 = 3 * GLA_KEY + GLA_VALUE + kv_width
    width2 = window_query.shape[1] + GLA_VALUE
    anyspec = pl.BlockSpec(memory_space=pl.ANY)
    vspec = pl.BlockSpec(memory_space=vm)
    result = pl.pallas_call(
        functools.partial(kernel, NS, NF, NT, tuple(levels)),
        out_shape=jax.ShapeDtypeStruct((length, depth), bf16),
        in_specs=[anyspec] * 9 + [vspec] * 5,
        out_specs=anyspec,
        scratch_shapes=[
            vm((NF, length, depth), bf16),
            vm((NZ, NY, NT, kb, width1), bf16),
            vm((NZ, NY, NT, kb, width2), bf16),
            vm((NF, linear_output.shape[0] + window_output.shape[0], depth), bf16),
            vm((len(levels) + 2, length, length), bf16),
            vm((NF, length, 2 * GLA_KEY), bf16),
            vm((NF, length, GLA_KEY), bf16),
            vm((NF, length, GLA_VALUE), bf16),
            vm((NF, length, GLA_KEY), bf16),
            vm((NF, length + WINDOW, kv_width), bf16),
            vm((NF, NZ, GLA_KEY // NZ, GLA_VALUE + 128), bf16),
            vm((NS, GLA_KEY // NZ, GLA_VALUE + 128), bf16),
            vm((NS, GLA_KEY // NZ, GLA_VALUE), bf16),
            vm((NF, NZ, GLA_KEY // NZ, GLA_VALUE), bf16),
            vm((NF, length, GLA_VALUE), bf16),
            vm((NF, length, window_query.shape[1]), bf16),
            vm((NF, length, GLA_VALUE), bf16),
            vm((NF, length, window_query.shape[1]), bf16),
            vm((NF, length, GLA_VALUE), f32),
            vm((NF, length, GLA_KEY), bf16),
            vm((NF, length, GLA_VALUE), bf16),
            vm((length, depth), f32),
            vm((length, depth), bf16),
            vm((6, 128, 192), f32),
            vm((6, 128, 192), bf16),
            dma((9,)),
            dma((3,)), dma((NZ // 2 + 2,)),
            dma((3,)), dma((2, NZ // 2 + 4)),
            dma((3,)),
            dma((4,)), dma((4,)),
            dma((1,)), dma((5,)),
            dma((1,)), dma((1,)),
            dma((1,)), dma((1,)),
            dma((1,)), dma((NF,)),
            dma((1,)), dma((1,)),
            dma((1,)), dma((1,)),
            dma((1,)), dma((1,)),
            dma((1,)), dma((3,)),
        ],
        compiler_params=pltpu.CompilerParams(
            collective_id=0, has_side_effects=True, vmem_limit_bytes=60 * 1024 * 1024),
        name="layer",
    )(tokens[0], linear_decay, linear_key, linear_value, linear_query, window_query, linear_gate,
      linear_output, window_output, window_key, window_value,
      decay_bias[None], norm_gain[None], sink_logit[None])
    return result[None]


def solution(mesh):
    shape = mesh.shape
    return jax.shard_map(
        functools.partial(shards, shape["sp"], shape["fs"], shape["tp"]),
        mesh=mesh,
        in_specs=(
            P(("fs", "tp"), "sp", None),
            P(("sp", "tp"), "fs"),
            P(("sp", "tp"), "fs"),
            P(("sp", "tp"), "fs"),
            P(("sp", "tp"), "fs"),
            P(("sp", "tp"), "fs"),
            P("fs"),
            P(),
            P(("sp", "tp"), "fs"),
            P(("sp", "tp"), "fs"),
            P(("sp", "tp"), "fs"),
            P("fs"),
            P("fs", None),
            P("fs", None),
        ),
        out_specs=P(("fs", "tp"), "sp", None),
        check_vma=False,
    )
```

time: 76.4 us -> 78.1 us (1.022)
  Pallas kernels: 74 us -> 75.7 us
    pallas_call x1, Pallas kernels: 74 us -> 75.7 us  [shards(): pl.pallas_call(functools.partial(kernel, NS, NF, NT, tuple(levels)), out_...]
where the time goes in v4:
time: 78.1 us; the launch traced here: 77.8 us
  Pallas kernels  75.7 us (97%)
  local copies, waits for them, and re-layouts  2.09 us (3%)
    pallas_call x1, Pallas kernels, shards(): pl.pallas_call(functools.partial(kernel, NS, NF, NT, tuple(levels)), out_...  75.7 us
    unnamed x1, local copies, waits for them, and re-layouts  2.09 us

profile of v4, /device:TPU:1, one launch (start us, length us, event | category | flops | bytes accessed | tf_op | source)
XLA Modules:
  0.0 77.8 jit_solution(5318557345702751064)
XLA Ops:
  0.0 75.7 %layer.1 = bf16[192,2048]{1,0:T(8,128)(2,1)} custom-call(bf16[192,2048]{1,0:T(8,128)(2,1)} %bitcast.6, bf16[32,128]{1,0:T(8,128)(2,1)} %w_decay.1, bf16[32,128]{1,0:T(8,128)(2,1)} %w_key.1, bf16[32,256]{1,0:T(8,128)(2,1)} %w_value.1, bf16[32,128]{1,0:T(8,128)(2,1)} %w_lq.1, bf16[32,256]{1,0:T(8,128)(2,1)} %w_wq.1, bf16[32,256]{1,0:T(8,128)(2,1)} %w_gate.1, ...), custom_call_target="tpu_custom_call" | custom-call | tf_op jit(solution)/shard_map/layer/pallas_call | solution.py:591
  75.7 2.1 %copy.16 = bf16[1,192,2048]{2,1,0:T(8,128)(2,1)} copy(bf16[1,192,2048]{2,1,0:T(8,128)(2,1)} %bitcast.5) | data formatting | bytes 1572864

commit v5 on v4

--- a/solution.py
+++ b/solution.py
@@ -13,6 +13,7 @@
 WINDOW = 128
 NY = 4
 XR = 128
+ZF = 128
 
 norm_epsilon = 1e-05
 MESH = pl.DeviceIdType.MESH
@@ -37,7 +38,7 @@
     out,
     toks, W1, W2, OW, sums, f2, kkey, val, query, kvbuf, lst, arr, pre, state_in,
     lrow, wrow, lall, wall, oacc, reach, gates, acc, obuf, sc, eb,
-    lsem, zs, zr, ys, yr, rr, dsnd, drcv, ts, tr, hs, hr, asnd, arcv, qs, qr,
+    lsem, zs, zr, zrr, ys, yr, rr, dsnd, drcv, ts, tr, hs, hr, asnd, arcv, qs, qr,
     ls, lr, ws, wr, xs, xr, os, orr,
 ):
     sp, f, t = lax.axis_index("sp"), lax.axis_index("fs"), lax.axis_index("tp")
@@ -74,7 +75,7 @@
         rc(ref, ref, sem, sem, other).wait_send()
 
     barrier = pltpu.get_barrier_semaphore()
-    greet = [at_z(d) for d in range(1, NZ)] + [at_y(1), at_y(NY - 1)] + [at_f(d) for d in range(1, NF)] + [other]
+    greet = [at_z(d) for d in range(1, NZ)] + [at_y(d) for d in range(1, NY)] + [at_f(d) for d in range(1, NF)] + [other]
     for dev in greet:
         pl.semaphore_signal(barrier, inc=1, device_id=dev, device_id_type=MESH)
     own1, own2 = W1.at[zz, yy, t], W2.at[zz, yy, t]
@@ -108,7 +109,7 @@
         kvbuf[:, 0:WINDOW, :] = jnp.zeros((NF, WINDOW, kvbuf.shape[2]), bf16)
 
     with scope("a_loads"):
-        for c in local:
+        for c in local[:7]:
             c.wait()
     with scope("b_barrier"):
         pl.semaphore_wait(barrier, len(greet))
@@ -139,31 +140,34 @@
         rc(ow_part(src, first), ow_part(dst, first), os.at[0], orr.at[min(j, 2)],
            at_f(1 if right else NF - 1)).start()
 
-    ow_x = OW.at[pl.ds(1, NF - 1), pl.ds(ZR, XR), cols_t]
-    tile_r = ZR // NZ
     tile_c = ocols // NY
+    region = {2: (ZR - ZF, ZF // NZ), 3: (0, (ZR - ZF) // NZ)}
+    others = pl.ds(1, NF - 1)
+    ow_x = OW.at[others, pl.ds(ZR, XR), cols_t]
 
     def ow_cols(yo):
         y1 = lax.rem(yy + NY - yo, NY)
         return pl.ds(pl.multiple_of(t * ocols + y1 * tile_c, tile_c), tile_c)
 
-    def ow_rows(z, count):
-        return pl.ds(pl.multiple_of(z * tile_r, tile_r), count * tile_r)
+    def ow_rows(g, z, count):
+        first, tile = region[g]
+        start = first + z * tile
+        return pl.ds(start if isinstance(z, int) else pl.multiple_of(start, tile), count * tile)
 
     def shard(g, k, yo):
         z1 = lax.rem(zz - k + NZ, NZ)
         if g == 2:
-            return OW.at[pl.ds(1, NF - 1), ow_rows(z1, 1), ow_cols(yo)]
+            return OW.at[others, ow_rows(2, z1, 1), ow_cols(yo)]
         return groups[g].at[z1, lax.rem(yy - yo + NY, NY), t]
 
     def box(g, z, count, yo):
         if g == 2:
-            return OW.at[pl.ds(1, NF - 1), pl.ds(z * tile_r, count * tile_r), ow_cols(yo)]
+            return OW.at[others, ow_rows(2, z, count), ow_cols(yo)]
         return groups[g].at[pl.ds(z, count), lax.rem(yy - yo + NY, NY), t]
 
     def whole(g, ycount):
         if g == 2:
-            return OW.at[pl.ds(1, NF - 1), pl.ds(0, ZR), pl.ds(0, ycount * tile_c)]
+            return OW.at[others, ow_rows(2, 0, NZ), pl.ds(0, ycount * tile_c)]
         return groups[g].at[:, pl.ds(0, ycount), t]
 
     pairs = [[0]] + [[d, NZ - d] for d in range(1, HZ)] + [[HZ]]
@@ -172,7 +176,7 @@
     left, right = 1, NY - 1
 
     def y_sem(g, side, part):
-        return yr.at[side, part if g == 0 else (ZW if g == 1 else ZW + 1 + part)]
+        return yr.at[side, part if g == 0 else ZW + g]
 
     def z_send(g):
         ref = shard(g, 0, 0)
@@ -201,14 +205,51 @@
         got(box(g, 0, NZ, 2), rr.at[g])
         core_box(g, 2)
 
-    def slice_send(d):
-        r, c = ow_rows(zz, 1), ow_cols(0)
-        rc(OW.at[0, r, c], OW.at[NF - d, r, c], xs.at[0], xr.at[0], at_f(d)).start()
-
-    slices = OW.at[pl.ds(1, NF - 1), ow_rows(zz, 1), ow_cols(0)]
-
-    for d in range(1, NF):
-        slice_send(d)
+    def slice_send(g, d):
+        r, c = ow_rows(g, zz, 1), ow_cols(0)
+        src = lin_o if g == 3 else win_o
+        r0 = pl.ds(pl.multiple_of(zz * region[g][1], region[g][1]), region[g][1])
+        rc(src.at[r0, c], OW.at[NF - d, r, c], xs.at[g - 2], xr.at[g - 2], at_f(d)).start()
+
+    def slices(g):
+        return OW.at[others, ow_rows(g, zz, 1), ow_cols(0)]
+
+    def ring_block(d):
+        return OW.at[others, ow_rows(3, lax.rem(zz + d + NZ, NZ), 1), cols_t]
+
+    def ring_half(d, up):
+        cols = pl.ds(pl.multiple_of(t * ocols + (0 if up else ocols // 2), ocols // 2), ocols // 2)
+        return OW.at[others, ow_rows(3, lax.rem(zz + d + NZ, NZ), 1), cols]
+
+    def ring_spread():
+        ref = slices(3)
+        for d in range(1, NY):
+            rc(ref, ref, ys.at[3], yr.at[0, ZW], at_y(d)).start()
+
+    def ring_ref(s, up):
+        d = -s if up else s
+        return ring_half(d, up) if s == HZ - 1 else ring_block(d)
+
+    def ring_step(s):
+        if s == 0:
+            got(OW.at[others, ow_rows(3, zz, 1), pl.ds(0, (NY - 1) * tile_c)], yr.at[0, ZW])
+            core_send(4, ring_block(0))
+        for up in (True, False):
+            if s > 0:
+                got(ring_ref(s - 1, up), zrr.at[0 if up else 1, s - 1])
+            if s < HZ:
+                ref = ring_ref(s, up)
+                rc(ref, ref, zs.at[3], zrr.at[0 if up else 1, s], at_z(1 if up else NZ - 1)).start()
+            if 0 < s < HZ:
+                core_send(4, ring_block(-s if up else s))
+        if s == HZ:
+            core_send(4, ring_block(HZ))
+
+    ring_all = OW.at[others, ow_rows(3, 0, NZ), cols_t]
+
+    for g in (3, 2):
+        for d in range(1, NF):
+            slice_send(g, d)
     z_send(0)
     for j in range(2):
         token_send(j)
@@ -216,6 +257,9 @@
     for j in range(2, 4):
         token_send(j)
     z_send(1)
+    with scope("c_slices"):
+        got(slices(3), xr.at[1])
+        ring_spread()
     with scope("c_z0"):
         for p in range(1, ZW):
             got(box(0, 0, len(pairs[p]), 0), zr.at[p - 1])
@@ -226,9 +270,12 @@
         for j in range(2):
             got(token_part(f, True), tr.at[j])
             token_send(4 + j)
-    with scope("d_slices"):
-        got(slices, xr.at[0])
+    with scope("d_ring0"):
+        ring_step(0)
+        got(slices(2), xr.at[0])
     z_send(2)
+    for c in local[7:]:
+        c.wait()
     for j in range(4):
         ow_send(j)
     with scope("e_y0"):
@@ -249,25 +296,13 @@
     with scope("g_core0"):
         got(whole(0, NY), drcv.at[0])
 
-    def y_arrive1():
-        got(box(1, 0, NZ, 0), y_sem(1, 0, 0))
-        relay(1, box(1, 0, HZ, left), True)
-        core_box(1, left)
-        got(box(1, 0, NZ, 0), y_sem(1, 1, 0))
-        relay(1, box(1, HZ, HZ, right), False)
-        core_box(1, right)
-
-    def y_arrive2(part):
-        if part == 0:
-            got(box(2, 0, HZ, 0), y_sem(2, 0, 0))
-            relay(2, box(2, 0, HZ, left), True)
-            got(box(2, 0, HZ, 0), y_sem(2, 1, 0))
-        else:
-            got(box(2, 0, HZ, 0), y_sem(2, 1, 1))
-            relay(2, box(2, HZ, HZ, right), False)
-            got(box(2, 0, HZ, 0), y_sem(2, 0, 1))
-            core_box(2, left)
-            core_box(2, right)
+    def y_arrive(g):
+        got(box(g, 0, NZ, 0), y_sem(g, 0, 0))
+        relay(g, box(g, 0, HZ, left), True)
+        core_box(g, left)
+        got(box(g, 0, NZ, 0), y_sem(g, 1, 0))
+        relay(g, box(g, HZ, HZ, right), False)
+        core_box(g, right)
 
     def order(i):
         return lax.rem(f + jnp.where(i == 0, 0, jnp.where(i == 1, NF - 1, i - 1)), NF)
@@ -278,6 +313,23 @@
 
     lane = lax.broadcasted_iota(jnp.int32, (LK, 128), 1)
 
+    def intra(b):
+        q = query[b].astype(f32) * LK ** -0.5
+        k = kkey[b].astype(f32)
+        ri = lax.broadcasted_iota(jnp.int32, (length, length), 0)
+        ci = lax.broadcasted_iota(jnp.int32, (length, length), 1)
+        rk = lax.broadcasted_iota(jnp.int32, (length, LK), 0)
+        scores = jnp.where(ri == ci, dot_t(q.astype(bf16), kkey[b]), 0.0)
+        for n, h in enumerate(levels):
+            decay = jnp.exp(log_sum(n, b))
+            later = (rk & h) != 0
+            qh = jnp.where(later, q * decay, 0.0).astype(bf16)
+            kh = jnp.where(later, 0.0, k * decay).astype(bf16)
+            same = (ri & ~(2 * h - 1)) == (ci & ~(2 * h - 1))
+            scores = scores + jnp.where(same, dot_t(qh, kh), 0.0)
+        reach[b] = (q * jnp.exp(log_sum(len(levels), b))).astype(bf16)
+        oacc[b] = dot(scores.astype(bf16), val[b])
+
     @pl.loop(0, NF)
     def _(i):
         b = order(i)
@@ -286,19 +338,22 @@
         def _():
             with scope("h_tok1"):
                 got(token_part(f, True), tr.at[2])
+            with scope("h_ring1"):
+                ring_step(1)
 
         @pl.when(i == 2)
         def _():
             with scope("h_tok2"):
                 got(token_part(f, True), tr.at[3])
             with scope("i_y1"):
-                y_arrive1()
+                y_arrive(1)
             with scope("i_z2"):
                 z_arrive(2)
-                pass_y(2, box(2, 0, HZ, 0), 0)
+                pass_y(2, box(2, 0, NZ, 0), 0)
 
         @pl.when(i == 3)
         def _():
+            intra(f)
             with scope("h_tok3"):
                 got(toks.at[f], tr.at[4])
 
@@ -334,40 +389,22 @@
 
         @pl.when(sp < NS - 1)
         def _():
-            rc(kvbuf.at[b, pl.ds(length, WINDOW)], kvbuf.at[b, pl.ds(0, WINDOW)], hs.at[0], hr.at[0],
+            rc(kvbuf.at[b, pl.ds(length, WINDOW)], kvbuf.at[b, pl.ds(0, WINDOW)], hs.at[0], hr.at[b],
                {"sp": lax.rem(sp + 1, NS)}).start()
 
-    pass_y(2, box(2, HZ, HZ, 0), 1)
-
-    @pl.loop(0, NF)
+    @pl.loop(1, NF)
     def _(i):
-        b = order(i)
-
-        @pl.when(i == 1)
+        @pl.when(i == 2)
         def _():
             with scope("i_relay1"):
                 relay_arrive(1)
 
         @pl.when(i == 3)
         def _():
-            with scope("i_y2"):
-                y_arrive2(0)
-
-        q = query[b].astype(f32) * LK ** -0.5
-        k = kkey[b].astype(f32)
-        ri = lax.broadcasted_iota(jnp.int32, (length, length), 0)
-        ci = lax.broadcasted_iota(jnp.int32, (length, length), 1)
-        rk = lax.broadcasted_iota(jnp.int32, (length, LK), 0)
-        scores = jnp.where(ri == ci, dot_t(q.astype(bf16), kkey[b]), 0.0)
-        for n, h in enumerate(levels):
-            decay = jnp.exp(log_sum(n, b))
-            later = (rk & h) != 0
-            qh = jnp.where(later, q * decay, 0.0).astype(bf16)
-            kh = jnp.where(later, 0.0, k * decay).astype(bf16)
-            same = (ri & ~(2 * h - 1)) == (ci & ~(2 * h - 1))
-            scores = scores + jnp.where(same, dot_t(qh, kh), 0.0)
-        reach[b] = (q * jnp.exp(log_sum(len(levels), b))).astype(bf16)
-        oacc[b] = dot(scores.astype(bf16), val[b])
+            with scope("h_ring2"):
+                ring_step(2)
+
+        intra(order(i))
 
     with scope("k_core1"):
         got(whole(1, NY), drcv.at[1])
@@ -414,15 +451,10 @@
     def rows_send(src, dst, ssem, rsem, off):
         rc(src.at[off], dst.at[lax.rem(NF - off, NF)], ssem.at[0], rsem.at[0], at_f(off)).start()
 
-    @pl.when(sp > 0)
-    def _():
-        with scope("k_halo"):
-            got(kvbuf.at[:, pl.ds(0, WINDOW)], hr.at[0])
-
     @pl.loop(0, NF)
     def _(i):
-        b = order(i)
-        off = lax.rem(b - f + NF, NF)
+        off = jnp.where(i == 0, NF - 1, jnp.where(i == NF - 1, 0, i))
+        b = lax.rem(f + off, NF)
 
         @pl.when(i == 2)
         def _():
@@ -431,7 +463,14 @@
         @pl.when(i == 3)
         def _():
             with scope("m_y2"):
-                y_arrive2(1)
+                y_arrive(2)
+            with scope("m_ring3"):
+                ring_step(3)
+
+        @pl.when(sp > 0)
+        def _():
+            with scope("k_halo"):
+                got(kvbuf.at[b, pl.ds(0, WINDOW)], hr.at[b])
 
         p = dot(toks[b], W2[...].reshape(depth, -1))
         gates[b] = p[:, wq:].astype(bf16)
@@ -474,51 +513,54 @@
             blocks.append(jnp.concatenate([res[:QB], res[QB:]], axis=1))
         win = jnp.concatenate(blocks, axis=0)
 
-        @pl.when(i == 0)
+        @pl.when(off == 0)
         def _():
             wall[0] = win
 
-        @pl.when(i > 0)
+        @pl.when(off > 0)
         def _():
             wrow[off] = win
             rows_send(wrow, wall, ws, wr, off)
+
+    @pl.loop(0, NF)
+    def _(i):
+        off = jnp.where(i == 0, 2, jnp.where(i == 1, NF - 1, jnp.where(i == 2, 1, 0)))
+        b = lax.rem(f + off, NF)
+
+        with scope("o_state"):
+            @pl.when(b != yy)
+            def _():
+                got(state_in.at[b], qr.at[b])
+
+            @pl.when(b == yy)
+            def _():
+                got(state_in.at[b, pl.ds(0, NZ - 1)], qr.at[b])
+
+        gate = gates[b].astype(f32)
+        o = oacc[b] + dot(reach[b], state_in[b].reshape(LK, GLA_VALUE))
+        scaled = o * lax.rsqrt(jnp.mean(o * o, axis=1, keepdims=True) + norm_epsilon)
+        lin = (scaled * gain[...] * (gate / (1.0 + jnp.exp(-gate)))).astype(bf16)
+
+        @pl.when(off == 0)
+        def _():
+            lall[0] = lin
+
+        @pl.when(off > 0)
+        def _():
+            lrow[off] = lin
+            rows_send(lrow, lall, ls, lr, off)
 
     with scope("n_ow"):
         relay_arrive(2)
         got(OW.at[pl.ds(1, 2), pl.ds(ZR, XR), cols_t], orr.at[2])
         core_send(3, ow_x)
-
-    @pl.loop(0, NF)
-    def _(i):
-        off = jnp.where(i == 0, 2, jnp.where(i == 1, NF - 1, jnp.where(i == 2, 1, 0)))
-        b = lax.rem(f + off, NF)
-
-        with scope("o_state"):
-            @pl.when(b != yy)
-            def _():
-                got(state_in.at[b], qr.at[b])
-
-            @pl.when(b == yy)
-            def _():
-                got(state_in.at[b, pl.ds(0, NZ - 1)], qr.at[b])
-
-        gate = gates[b].astype(f32)
-        o = oacc[b] + dot(reach[b], state_in[b].reshape(LK, GLA_VALUE))
-        scaled = o * lax.rsqrt(jnp.mean(o * o, axis=1, keepdims=True) + norm_epsilon)
-        lin = (scaled * gain[...] * (gate / (1.0 + jnp.exp(-gate)))).astype(bf16)
-
-        @pl.when(off == 0)
-        def _():
-            lall[0] = lin
-
-        @pl.when(off > 0)
-        def _():
-            lrow[off] = lin
-            rows_send(lrow, lall, ls, lr, off)
+    with scope("n_ring4"):
+        ring_step(4)
 
     with scope("p_ow"):
         got(whole(2, NY), drcv.at[2])
         got(ow_x, drcv.at[3])
+        got(ring_all, drcv.at[4])
     with scope("p_wrow"):
         got(wall.at[pl.ds(1, NF - 1)], wr.at[0])
 
@@ -549,7 +591,11 @@
     with scope("t_end"):
         gone(toks.at[pl.ds(0, NF - 1)], ts.at[0])
         gone(ow_x, os.at[0])
-        gone(slices, xs.at[0])
+        gone(slices(2), xs.at[0])
+        gone(slices(3), xs.at[1])
+        gone(OW.at[others, ow_rows(3, 0, 1), pl.ds(0, (NY - 1) * tile_c)], ys.at[3])
+        gone(OW.at[others, ow_rows(3, 0, NZ - 1), cols_t], zs.at[3])
+        gone(ring_all, dsnd.at[4])
         gone(wrow.at[pl.ds(1, NF - 1)], ws.at[0])
         gone(lrow.at[pl.ds(1, NF - 1)], ls.at[0])
         for g in range(3):
@@ -620,17 +666,17 @@
             vm((6, 128, 192), f32),
             vm((6, 128, 192), bf16),
             dma((9,)),
-            dma((3,)), dma((NZ // 2 + 2,)),
-            dma((3,)), dma((2, NZ // 2 + 4)),
+            dma((4,)), dma((NZ // 2 + 2,)), dma((2, NZ // 2)),
+            dma((4,)), dma((2, NZ // 2 + 4)),
             dma((3,)),
-            dma((4,)), dma((4,)),
+            dma((5,)), dma((5,)),
             dma((1,)), dma((5,)),
-            dma((1,)), dma((1,)),
+            dma((1,)), dma((NF,)),
             dma((1,)), dma((1,)),
             dma((1,)), dma((NF,)),
             dma((1,)), dma((1,)),
             dma((1,)), dma((1,)),
-            dma((1,)), dma((1,)),
+            dma((2,)), dma((2,)),
             dma((1,)), dma((3,)),
         ],
         compiler_params=pltpu.CompilerParams(

time: 78.1 us -> 74.2 us (0.950)
  Pallas kernels: 75.7 us -> 71.9 us
    pallas_call x1, Pallas kernels: 75.7 us -> 71.9 us  [shards(): pl.pallas_call(functools.partial(kernel, NS, NF, NT, tuple(levels)), out_...]
where the time goes in v5:
time: 74.2 us; the launch traced here: 74 us
  Pallas kernels  71.9 us (97%)
  local copies, waits for them, and re-layouts  2.09 us (3%)
    pallas_call x1, Pallas kernels, shards(): pl.pallas_call(functools.partial(kernel, NS, NF, NT, tuple(levels)), out_...  71.9 us
    unnamed x1, local copies, waits for them, and re-layouts  2.09 us

profile of v5, /device:TPU:1, one launch (start us, length us, event | category | flops | bytes accessed | tf_op | source)
XLA Modules:
  0.0 74.0 jit_solution(4771153420658043063)
XLA Ops:
  0.0 71.9 %layer.1 = bf16[192,2048]{1,0:T(8,128)(2,1)} custom-call(bf16[192,2048]{1,0:T(8,128)(2,1)} %bitcast.6, bf16[32,128]{1,0:T(8,128)(2,1)} %w_decay.1, bf16[32,128]{1,0:T(8,128)(2,1)} %w_key.1, bf16[32,256]{1,0:T(8,128)(2,1)} %w_value.1, bf16[32,128]{1,0:T(8,128)(2,1)} %w_lq.1, bf16[32,256]{1,0:T(8,128)(2,1)} %w_wq.1, bf16[32,256]{1,0:T(8,128)(2,1)} %w_gate.1, ...), custom_call_target="tpu_custom_call" | custom-call | tf_op jit(solution)/shard_map/layer/pallas_call | solution.py:637
  71.9 2.1 %copy.16 = bf16[1,192,2048]{2,1,0:T(8,128)(2,1)} copy(bf16[1,192,2048]{2,1,0:T(8,128)(2,1)} %bitcast.5) | data formatting | bytes 1572864
